TPU v7x, 128 devices: a whole 4x4x4 slice. The times are simulated.
128 devices in a mesh: sp: 16 (over z, y), dp: 8 (over x, core).
Axes of the slice: x: 4, y: 4, z: 4, core: 2. Of those that a mesh axis runs over, the one named last changes fastest.
Arguments:
- residual: bfloat16 [8, 2048, 2048], P('dp', 'sp'), may hold values from -6 to 6
- query: bfloat16 [8, 2048, 1536], P('dp', 'sp'), may hold values from -64 to 64
- latent: bfloat16 [8, 2048, 256], P('dp', 'sp'), may hold values from -6 to 6
- rope_key: bfloat16 [8, 2048, 32], P('dp', 'sp'), may hold values from -64 to 64
- latent_gain: float32 [256], replicated, may hold values from 0.1 to 1.9
- query_gain: float32 [96], replicated, may hold values from 0.7 to 5.6
- key_gain: float32 [96], replicated, may hold values from 0.7 to 5.6
- key_weight: bfloat16 [256, 1024], replicated, may hold values from -0.375 to 0.375
- value_weight: bfloat16 [256, 1024], replicated, may hold values from -0.375 to 0.375
- mix_gain: float32 [1024], replicated, may hold values from 0.1 to 1.9
- out_weight: bfloat16 [1024, 2048], replicated, may hold values from -0.1875 to 0.1875
- ffn_gain: float32 [2048], replicated, may hold values from 0.1 to 1.9
- expert_choice: int32 [8, 2048, 2], P('dp', 'sp'), may hold values from 0 to 127, as said below
- group_prob: float32 [8, 2048], P('dp', 'sp'), may hold values from 0.25 to 1
- expert_prob: float32 [8, 2048, 2], P('dp', 'sp'), may hold values from 0.05 to 1
- gate_weight: bfloat16 [128, 2048, 512], P(('sp', 'dp')), may hold values from -0.125 to 0.125
- up_weight: bfloat16 [128, 2048, 512], P(('sp', 'dp')), may hold values from -0.125 to 0.125
- down_weight: bfloat16 [128, 512, 2048], P(('sp', 'dp')), may hold values from -0.25 to 0.25
Outputs:
- layer_out: bfloat16 [8, 2048, 2048], P('dp', 'sp')
Inputs may be any that keep to these rules, and one draw needn't show every extreme that they name: `expert_choice`: A token's two experts differ and lie in one group of 32 consecutive expert numbers. In each aligned block of 128 tokens (the tokens of one device) no expert is named more than 4 times, and every expert of one group is named exactly 4 times in every block.
All inputs are finite; a program needn't handle non-finite values.
Results may differ from a plain program's by a relative error of at most 0.012.
The roundings to bfloat16 on the way count: a program that leaves them out, or rounds other values in their place, can miss the bound.
Values may be sent and summed in bfloat16 or wider, within the bound.
No kernel may reach another device: no remote copies, remote signals or barrier semaphores. Data moves between devices by JAX's collectives and lax.ppermute only.
A program may use at most 64 MiB of HBM per device.

v0:
```python
import jax
import jax.numpy as jnp
from jax import lax
from jax.sharding import PartitionSpec as P

GROUPS = 4
SPAN = 64


eps = 1e-06


def sent_together(arrays, axis, split_dim, concat_dim, along):
    widths = [a.shape[along] for a in arrays]
    both = jnp.concatenate(arrays, axis=along)
    out = lax.all_to_all(both, axis, split_axis=split_dim, concat_axis=concat_dim, tiled=True)
    return tuple(jnp.split(out, [sum(widths[:k]) for k in range(1, len(widths))], axis=along))


def rms_scale(vector, gains):
    return vector * lax.rsqrt(jnp.mean(vector * vector, axis=-1, keepdims=True) + eps) * gains


def rotate(vector, phases):
    half_width = vector.shape[-1] // 2
    lower_half = vector[..., :half_width]
    upper_half = vector[..., half_width:]
    cos_table = jnp.cos(phases)
    sin_table = jnp.sin(phases)
    return jnp.concatenate(
        [
            lower_half * cos_table - upper_half * sin_table,
            upper_half * cos_table + lower_half * sin_table,
        ],
        axis=-1,
    )


def angles(offset, span_count, rope_width):
    position = (offset + jnp.arange(span_count, dtype=jnp.int32)).astype(jnp.float32)
    frequency = 10000.0 ** (-2.0 * jnp.arange(rope_width // 2, dtype=jnp.float32) / rope_width)
    return position[:, None] * frequency[None, :]


def head_vectors(nope_part, rope_part, gains, phases):
    normed_all = rms_scale(jnp.concatenate([nope_part, rope_part], axis=-1), gains)
    split_at = nope_part.shape[-1]
    turned = rotate(normed_all[..., split_at:], phases[:, None, :])
    return jnp.concatenate([normed_all[..., :split_at], turned], axis=-1).astype(jnp.bfloat16)


def attend(queries_head, keys_head, values_head):
    length = queries_head.shape[0]
    blocks_count = max(4, length // 1024)
    block_rows = length // blocks_count
    score_scale = queries_head.shape[-1] ** (-0.5)
    pieces = []
    for block_index in range(blocks_count):
        first_row = block_index * block_rows
        last_row = first_row + block_rows
        scores = (
            jnp.einsum(
                "qhd,khd->hqk",
                queries_head[first_row:last_row],
                keys_head[:last_row],
                preferred_element_type=jnp.float32,
            )
            * score_scale
        )
        query_pos = first_row + jnp.arange(block_rows, dtype=jnp.int32)
        key_pos = jnp.arange(last_row, dtype=jnp.int32)
        allowed = key_pos[None, :] // SPAN <= query_pos[:, None] // SPAN
        scores = jnp.where(allowed[None], scores, -1e30)
        row_top = jnp.max(scores, axis=-1, keepdims=True)
        raised = jnp.exp(scores - row_top)
        row_sum = jnp.sum(raised, axis=-1)
        summed = jnp.einsum(
            "hqk,khd->qhd",
            raised.astype(jnp.bfloat16),
            values_head[:last_row],
            preferred_element_type=jnp.float32,
        )
        pieces.append((summed / row_sum.T[:, :, None]).astype(jnp.bfloat16))
    return jnp.concatenate(pieces, axis=0)


def per_device(
    residual,
    query,
    latent,
    rope_key,
    latent_gain,
    query_gain,
    key_gain,
    key_weight,
    value_weight,
    mix_gain,
    out_weight,
    ffn_gain,
    expert_choice,
    group_prob,
    expert_prob,
    gate_weight,
    up_weight,
    down_weight,
):
    tok_rows = residual.shape[1]
    model_width = residual.shape[2]
    rope_width = rope_key.shape[2]
    qk_width = query_gain.shape[0]
    nope_width = qk_width - rope_width
    head_count = query.shape[2] // qk_width
    value_width = value_weight.shape[1] // head_count
    seq_devices = lax.axis_size("sp")
    offset = lax.axis_index("sp") * tok_rows
    own_phases = angles(offset, tok_rows, rope_width)
    raw_query = query[0].astype(jnp.float32).reshape(tok_rows, head_count, qk_width)
    queries_tok = head_vectors(
        raw_query[..., :nope_width], raw_query[..., nope_width:], query_gain, own_phases
    )
    normed_latent = rms_scale(latent[0].astype(jnp.float32), latent_gain).astype(jnp.bfloat16)
    key_part = jnp.dot(normed_latent, key_weight, preferred_element_type=jnp.float32).astype(
        jnp.bfloat16
    )
    values_tok = jnp.dot(normed_latent, value_weight, preferred_element_type=jnp.float32).astype(
        jnp.bfloat16
    )
    values_tok = values_tok.reshape(tok_rows, head_count, value_width)
    shared_rope = jnp.broadcast_to(
        rope_key[0].astype(jnp.float32)[:, None, :], (tok_rows, head_count, rope_width)
    )
    keys_tok = head_vectors(
        key_part.astype(jnp.float32).reshape(tok_rows, head_count, nope_width),
        shared_rope,
        key_gain,
        own_phases,
    )
    queries_head, keys_head, values_head = sent_together(
        (queries_tok, keys_tok, values_tok), "sp", 1, 0, 2
    )
    head_out = attend(queries_head, keys_head, values_head)
    token_out = lax.all_to_all(head_out, "sp", split_axis=0, concat_axis=1, tiled=True).reshape(
        tok_rows, head_count * value_width
    )
    mixed_in = rms_scale(token_out.astype(jnp.float32), mix_gain).astype(jnp.bfloat16)
    stream = residual[0].astype(jnp.float32) + jnp.dot(
        mixed_in, out_weight, preferred_element_type=jnp.float32
    )
    normed = rms_scale(stream, ffn_gain).astype(jnp.bfloat16)
    expert_total = seq_devices * lax.axis_size("dp")
    capacity = tok_rows * GROUPS // expert_total
    picked = expert_choice[0].reshape(-1)
    one_hot = (picked[:, None] == jnp.arange(expert_total, dtype=jnp.int32)[None, :]).astype(
        jnp.int32
    )
    earlier = jnp.cumsum(one_hot, axis=0) - one_hot
    slot_rank = jnp.sum(earlier * one_hot, axis=1)
    target = picked * capacity + slot_rank
    source_row = jnp.arange(picked.shape[0], dtype=jnp.int32) // expert_choice.shape[2]
    slot_token = (
        jnp.full((expert_total * capacity,), tok_rows, jnp.int32).at[target].set(source_row)
    )
    padded = jnp.concatenate([normed, jnp.zeros((1, model_width), jnp.bfloat16)], axis=0)
    outgoing = padded[slot_token].reshape(expert_total, capacity, model_width)
    arrived = lax.all_to_all(outgoing, ("sp", "dp"), split_axis=0, concat_axis=0, tiled=True)
    flat_rows = arrived.reshape(-1, model_width)
    gate_act = jnp.dot(flat_rows, gate_weight[0], preferred_element_type=jnp.float32)
    upward = jnp.dot(flat_rows, up_weight[0], preferred_element_type=jnp.float32)
    hidden = (jax.nn.silu(gate_act) * upward).astype(jnp.bfloat16)
    returned = lax.all_to_all(
        jnp.dot(hidden, down_weight[0], preferred_element_type=jnp.float32)
        .astype(jnp.bfloat16)
        .reshape(arrived.shape),
        ("sp", "dp"),
        split_axis=0,
        concat_axis=0,
        tiled=True,
    )
    gathered_rows = returned.reshape(-1, model_width)[target].reshape(
        tok_rows, expert_choice.shape[2], model_width
    )
    expert_share = expert_prob[0]
    route_weight = (
        group_prob[0][:, None] * expert_share / jnp.sum(expert_share, axis=-1, keepdims=True)
    )
    routed_sum = route_weight[:, 0:1] * gathered_rows[:, 0].astype(jnp.float32) + route_weight[
        :, 1:2
    ] * gathered_rows[:, 1].astype(jnp.float32)
    return (stream + routed_sum).astype(jnp.bfloat16)[None]


def solution(mesh):
    return jax.shard_map(
        per_device,
        mesh=mesh,
        in_specs=(
            P("dp", "sp", None),
            P("dp", "sp", None),
            P("dp", "sp", None),
            P("dp", "sp", None),
            P(),
            P(),
            P(),
            P(),
            P(),
            P(),
            P(),
            P(),
            P("dp", "sp", None),
            P("dp", "sp"),
            P("dp", "sp", None),
            P(("sp", "dp"), None, None),
            P(("sp", "dp"), None, None),
            P(("sp", "dp"), None, None),
        ),
        out_specs=P("dp", "sp", None),
        check_vma=False,
    )
```

profile of v0, /device:TPU:1, one launch (start us, length us, event | category | flops | bytes accessed | tf_op | source)
XLA Modules:
  0.0 179.6 jit_solution(8761957602217272997)
XLA Ops:
  0.0 1.4 copy.120
  4.7 1.3 fusion.25
  9.8 8.6 %all-to-all-start = ((bf16[128,16,256]{0,2,1:T(8,128)(2,1)}), bf16[128,16,256]{0,2,1:T(8,128)(2,1)S(1)}, u32[]{:S(2)}, u32[]{:S(2)}) async-start(bf16[128,16,256]{0,2,1:T(8,128)(2,1)} %constant_dynamic-update-slice_fusion), calls=%async_computation | async-start | bytes 2097152 | tf_op jit(solution)/shard_map/all_to_all | solution.py:16
  19.7 1.4 scatter_custom_fusion
  21.2 13.3 %all-to-all-done = bf16[128,16,256]{0,2,1:T(8,128)(2,1)S(1)} async-done(((bf16[128,16,256]{0,2,1:T(8,128)(2,1)}), bf16[128,16,256]{0,2,1:T(8,128)(2,1)S(1)}, u32[]{:S(2)}, u32[]{:S(2)}) %all-to-all-start) | async-done | bytes 1048608 | tf_op jit(solution)/shard_map/all_to_all | solution.py:16
  35.5 1.5 copy.123
  43.7 1.2 fusion.44
  47.6 4.2 %all-to-all-start.1 = ((bf16[16,2,4096]{2,1,0:T(2,128)(2,1)}), bf16[16,2,4096]{2,1,0:T(2,128)(2,1)S(1)}, u32[]{:S(2)}, u32[]{:S(2)}) async-start(bf16[16,2,4096]{2,1,0:T(2,128)(2,1)} %reshape.671), calls=%async_computation.1 | async-start | bytes 524288 | tf_op jit(solution)/shard_map/all_to_all | solution.py:142
  51.8 7.6 %all-to-all-done.1 = bf16[16,2,4096]{2,1,0:T(2,128)(2,1)S(1)} async-done(((bf16[16,2,4096]{2,1,0:T(2,128)(2,1)}), bf16[16,2,4096]{2,1,0:T(2,128)(2,1)S(1)}, u32[]{:S(2)}, u32[]{:S(2)}) %all-to-all-start.1) | async-done | bytes 262176 | tf_op jit(solution)/shard_map/all_to_all | solution.py:142
  61.7 3.0 %multiply_reduce_fusion = (f32[128]{0:T(128)S(1)}, f32[128,2048]{1,0:T(8,128)S(1)}) fusion(bf16[128,1024]{0,1:T(8,128)(2,1)S(1)} %fusion.71, bf16[1024,2048]{1,0:T(8,128)(2,1)} %param.28, bf16[1,128,2048]{2,1,0:T(8,128)(2,1)S(1)} %copy-done.5), kind=kOutput, calls=%fused_computation.56 | convolution fusion | flops 537919360 | bytes 6029824 | tf_op jit(solution)/shard_map/dot_general | solution.py:146
  65.9 3.3 %gather_fusion = bf16[512,2048]{1,0:T(8,128)(2,1)} fusion(bf16[129,2048]{1,0:T(8,128)(2,1)S(1)} %concatenate.21, s32[1024]{0:T(1024)S(1)} %pad_clamp_fusion.1), kind=kCustom, calls=%fused_computation | custom fusion | bytes 4196352 | tf_op jit(solution)/shard_map/gather | solution.py:164
  69.2 4.1 %reshape.628 = bf16[128,4,2048]{2,1,0:T(4,128)(2,1)} reshape(bf16[512,2048]{1,0:T(8,128)(2,1)} %gather_fusion) | data formatting | bytes 4194304 | tf_op jit(solution)/shard_map/reshape | solution.py:164
  73.3 38.6 %all_to_all.37 = bf16[128,4,2048]{2,1,0:T(4,128)(2,1)} all-to-all(bf16[128,4,2048]{2,1,0:T(4,128)(2,1)} %reshape.628), channel_id=1, replica_groups=mesh['sp'=16,'dp'=8] {'sp','dp'}, dimensions={0} | all-to-all | bytes 4194304 | tf_op jit(solution)/shard_map/all_to_all | solution.py:165
  111.9 4.0 %reshape.629 = bf16[512,2048]{1,0:T(8,128)(2,1)} reshape(bf16[128,4,2048]{2,1,0:T(4,128)(2,1)} %all_to_all.37) | data formatting | bytes 4194304 | tf_op jit(solution)/shard_map/reshape | solution.py:166
  115.9 3.5 %fusion.10 = f32[512,512]{1,0:T(8,128)S(1)} fusion(bf16[512,2048]{1,0:T(8,128)(2,1)} %reshape.629, bf16[1,2048,512]{2,1,0:T(8,128)(2,1)} %param.33), kind=kOutput, calls=%fused_computation.18 | convolution fusion | flops 1073741824 | bytes 5242880 | tf_op jit(solution)/shard_map/dot_general | solution.py:167
  119.4 6.0 %convolution_convert_fusion = bf16[512,2048]{1,0:T(8,128)(2,1)} fusion(bf16[1,512,2048]{2,1,0:T(8,128)(2,1)S(1)} %copy-done, bf16[512,2048]{1,0:T(8,128)(2,1)} %reshape.629, bf16[1,2048,512]{2,1,0:T(8,128)(2,1)} %param.34, f32[512,512]{1,0:T(8,128)S(1)} %fusion.10), kind=kOutput, calls=%fused_computation.10 | convolution fusion | flops 2150105088 | bytes 9437184 | tf_op jit(solution)/shard_map/dot_general | solution.py:171
  125.3 4.1 %reshape.630 = bf16[128,4,2048]{2,1,0:T(4,128)(2,1)} reshape(bf16[512,2048]{1,0:T(8,128)(2,1)} %convolution_convert_fusion) | data formatting | bytes 4194304 | tf_op jit(solution)/shard_map/reshape | solution.py:173
  129.5 5.6 %all-to-all-start.3 = ((bf16[128,4,2048]{2,1,0:T(4,128)(2,1)}), bf16[128,4,2048]{2,1,0:T(4,128)(2,1)}, u32[]{:S(2)}, u32[]{:S(2)}) async-start(bf16[128,4,2048]{2,1,0:T(4,128)(2,1)} %reshape.630), calls=%async_computation.3 | async-start | bytes 4194304 | tf_op jit(solution)/shard_map/all_to_all | solution.py:170
  135.1 30.2 %all-to-all-done.3 = bf16[128,4,2048]{2,1,0:T(4,128)(2,1)} async-done(((bf16[128,4,2048]{2,1,0:T(4,128)(2,1)}), bf16[128,4,2048]{2,1,0:T(4,128)(2,1)}, u32[]{:S(2)}, u32[]{:S(2)}) %all-to-all-start.3) | async-done | bytes 2097184 | tf_op jit(solution)/shard_map/all_to_all | solution.py:170
  165.3 4.0 %reshape.631 = bf16[512,2048]{1,0:T(8,128)(2,1)} reshape(bf16[128,4,2048]{2,1,0:T(4,128)(2,1)} %all-to-all-done.3) | data formatting | bytes 4194304 | tf_op jit(solution)/shard_map/reshape | solution.py:179
  169.3 5.2 %gather_fusion.1 = bf16[256,2048]{1,0:T(8,128)(2,1)} fusion(bf16[512,2048]{1,0:T(8,128)(2,1)} %reshape.631, s32[1024]{0:T(1024)S(1)} %pad_clamp_fusion), kind=kCustom, calls=%fused_computation.1 | custom fusion | bytes 2098176 | tf_op jit(solution)/shard_map/gather | solution.py:179
  174.5 1.7 reshape.632
  176.3 1.5 fusion.115
  177.8 1.9 %fusion.69 = bf16[1,128,2048]{2,1,0:T(8,128)(2,1)} fusion(f32[128,2048]{1,0:T(8,128)S(1)} %copy-done.2, bf16[128,1,2048]{2,1,0:T(2,128)(2,1)S(1)} %get-tuple-element.6, bf16[128,1,2048]{2,1,0:T(2,128)(2,1)S(1)} %get-tuple-element.5, f32[128]{0:T(128)S(1)} %get-tuple-element.8, f32[128]{0:T(128)S(1)} %get-tuple-element.7), kind=kLoop, calls=%fused_computation.71 | loop fusion | flops 1835008 | bytes 2622464 | tf_op jit(solution)/shard_map/broadcast_in_dim | solution.py:189
  (111 shorter events, 22.1 us)
Async XLA Ops:
  0.0 119.4 %copy-start = (bf16[1,512,2048]{2,1,0:T(8,128)(2,1)S(1)}, bf16[1,512,2048]{2,1,0:T(8,128)(2,1)}, u32[]{:S(2)}) copy-start(bf16[1,512,2048]{2,1,0:T(8,128)(2,1)} %param.35) | copy-start | bytes 6291460
  0.0 4.5 %copy-start.4 = (bf16[1,128,256]{2,1,0:T(8,128)(2,1)S(1)}, bf16[1,128,256]{2,1,0:T(8,128)(2,1)}, u32[]{:S(2)}) copy-start(bf16[1,128,256]{2,1,0:T(8,128)(2,1)} %param.20) | copy-start | bytes 196612
  0.0 4.7 %copy-start.10 = (f32[256]{0:T(256)S(1)}, f32[256]{0:T(256)}, u32[]{:S(2)}) copy-start(f32[256]{0:T(256)} %param.22) | copy-start | bytes 3076
  1.5 4.7 %copy-start.8 = (bf16[1,128,32]{1,2,0:T(8,128)(2,1)S(1)}, bf16[1,128,32]{1,2,0:T(8,128)(2,1)}, u32[]{:S(2)}) copy-start(bf16[1,128,32]{1,2,0:T(8,128)(2,1)} %param.21) | copy-start | bytes 24580
  3.1 3.2 %copy-start.13 = (f32[96]{0:T(128)S(1)}, f32[96]{0:T(128)}, u32[]{:S(2)}) copy-start(f32[96]{0:T(128)} %param.24) | copy-start | bytes 1156
  6.2 2.4 %copy-start.6 = (bf16[256,1024]{1,0:T(8,128)(2,1)S(1)}, bf16[256,1024]{1,0:T(8,128)(2,1)}, u32[]{:S(2)}) copy-start(bf16[256,1024]{1,0:T(8,128)(2,1)} %param.26) | copy-start | bytes 1572868
  8.0 10.5 %copy-start.11 = (s32[1,128,2]{1,2,0:T(2,128)S(1)}, s32[1,128,2]{1,2,0:T(2,128)}, u32[]{:S(2)}) copy-start(s32[1,128,2]{1,2,0:T(2,128)} %param.30) | copy-start | bytes 3076
  9.8 24.6 %all-to-all-start = ((bf16[128,16,256]{0,2,1:T(8,128)(2,1)}), bf16[128,16,256]{0,2,1:T(8,128)(2,1)S(1)}, u32[]{:S(2)}, u32[]{:S(2)}) async-start(bf16[128,16,256]{0,2,1:T(8,128)(2,1)} %constant_dynamic-update-slice_fusion), calls=%async_computation | async-start | bytes 2097152 | tf_op jit(solution)/shard_map/all_to_all | solution.py:16
  34.5 1.0 copy-start.3
  47.6 11.8 %all-to-all-start.1 = ((bf16[16,2,4096]{2,1,0:T(2,128)(2,1)}), bf16[16,2,4096]{2,1,0:T(2,128)(2,1)S(1)}, u32[]{:S(2)}, u32[]{:S(2)}) async-start(bf16[16,2,4096]{2,1,0:T(2,128)(2,1)} %reshape.671), calls=%async_computation.1 | async-start | bytes 524288 | tf_op jit(solution)/shard_map/all_to_all | solution.py:142
  60.0 1.1 copy-start.9
  60.6 1.0 copy-start.5
  61.7 4.0 %copy-start.7 = (f32[2048]{0:T(1024)S(1)}, f32[2048]{0:T(1024)}, u32[]{:S(2)}) copy-start(f32[2048]{0:T(1024)} %param.29) | copy-start | bytes 24580
  64.7 1.0 copy-start.1
  129.5 5.6 %copy-start.12 = (f32[1,128,2]{1,2,0:T(2,128)S(1)}, f32[1,128,2]{1,2,0:T(2,128)}, u32[]{:S(2)}) copy-start(f32[1,128,2]{1,2,0:T(2,128)} %param.32) | copy-start | bytes 3076
  129.5 5.7 %copy-start.14 = (f32[1,128]{1,0:T(1,128)S(1)}, f32[1,128]{1,0:T(1,128)}, u32[]{:S(2)}) copy-start(f32[1,128]{1,0:T(1,128)} %param.31) | copy-start | bytes 1540
  129.5 35.9 %all-to-all-start.3 = ((bf16[128,4,2048]{2,1,0:T(4,128)(2,1)}), bf16[128,4,2048]{2,1,0:T(4,128)(2,1)}, u32[]{:S(2)}, u32[]{:S(2)}) async-start(bf16[128,4,2048]{2,1,0:T(4,128)(2,1)} %reshape.630), calls=%async_computation.3 | async-start | bytes 4194304 | tf_op jit(solution)/shard_map/all_to_all | solution.py:170
  176.2 1.5 copy-start.2
where the time goes:
time: 181 us; the launch traced here: 180 us
  waiting for transfers between devices  51 us (28%)
  local copies, waits for them, and re-layouts  41.5 us (23%)
  blocking collectives  38.6 us (21%)
  matrix products  20 us (11%)
  starting transfers between devices  18.4 us (10%)
  other arithmetic  9.68 us (5%)
    all_to_all x1, blocking collectives, per_device(): lax.all_to_all(outgoing, ('sp', 'dp'), split_axis=0, concat_axis=0, tiled...  38.6 us
    all_to_all x1, waiting for transfers between devices, per_device(): lax.all_to_all(jnp.dot(hidden, down_weight[0], preferred_element_type=jnp...  30.2 us
    all_to_all x1, waiting for transfers between devices, sent_together(): lax.all_to_all(both, axis, split_axis=split_dim, concat_axis=concat_dim,...  13.3 us
    all_to_all x1, starting transfers between devices, sent_together(): lax.all_to_all(both, axis, split_axis=split_dim, concat_axis=concat_dim,...  8.59 us
    unnamed x39, local copies, waits for them, and re-layouts  7.56 us
    all_to_all x1, waiting for transfers between devices, per_device(): lax.all_to_all(head_out, 'sp', split_axis=0, concat_axis=1, tiled=True)  7.55 us
    dot_general x1, matrix products, per_device(): jnp.dot(hidden, down_weight[0], preferred_element_type=jnp.float32)  5.96 us
    reshape x2, local copies, waits for them, and re-layouts, per_device(): returned.reshape(-1, model_width)[target]  5.71 us
  transfers between devices with their start and end apart: 3, of which 3 were waited for; matrix products, arithmetic and copies ran while one was open for 2% of the time, Pallas kernels for 0%

commit v1 on v0

v1 whole, which is shorter than its diff:
```python
import jax
import jax.numpy as jnp
from jax import lax
from jax.experimental import pallas as pl
from jax.experimental.pallas import tpu as pltpu
from jax.sharding import PartitionSpec as P

SPAN = 64
LANES = 128
SLOTS = 4

eps = 1e-06


def angles(offset, span_count, rope_width):
    position = (offset + jnp.arange(span_count, dtype=jnp.int32)).astype(jnp.float32)
    frequency = 10000.0 ** (-2.0 * jnp.arange(rope_width // 2, dtype=jnp.float32) / rope_width)
    return position[:, None] * frequency[None, :]


def lane_iota(rows, width=LANES):
    return lax.broadcasted_iota(jnp.int32, (rows, width), 1)


def inverse_rms(vector, width):
    return lax.rsqrt(jnp.sum(vector * vector, axis=-1, keepdims=True) * (1.0 / width) + eps)


def project_kernel(query, latent, rope, latent_gain, gains, turn, key_weight, value_weight, out):
    rows = query.shape[0]
    heads = query.shape[1] // 96
    lane = lane_iota(rows)
    raw_latent = latent[...].astype(jnp.float32)
    normed_latent = (
        raw_latent * inverse_rms(raw_latent, raw_latent.shape[1]) * latent_gain[...]
    ).astype(jnp.bfloat16)
    key_part = (
        jnp.dot(normed_latent, key_weight[...], preferred_element_type=jnp.float32)
        .astype(jnp.bfloat16)
        .astype(jnp.float32)
    )
    values = jnp.dot(normed_latent, value_weight[...], preferred_element_type=jnp.float32)
    place = (
        lax.broadcasted_iota(jnp.int32, (32, LANES), 0) + 64 == lane_iota(32)
    ).astype(jnp.bfloat16)
    rope_part = jnp.dot(rope[...], place, preferred_element_type=jnp.float32)
    cos_part = turn[:, 0:128]
    minus_sin = turn[:, 128:256]
    plus_sin = turn[:, 256:384]

    def finish(vector, gain):
        scaled = vector * inverse_rms(vector, 96) * gain
        return (
            scaled * cos_part
            + pltpu.roll(scaled, 112, 1) * minus_sin
            + pltpu.roll(scaled, 16, 1) * plus_sin
        )

    for head in range(heads):
        first = head * 96
        tile, shift = first // 128, first % 128
        here = query[:, tile * 128 : tile * 128 + 128].astype(jnp.float32)
        if shift:
            here = pltpu.roll(here, 128 - shift, 1)
        if shift > 32:
            after = query[:, tile * 128 + 128 : tile * 128 + 256].astype(jnp.float32)
            here = jnp.where(lane < 128 - shift, here, pltpu.roll(after, 128 - shift, 1))
        raw_query = jnp.where(lane < 96, here, 0.0)
        pair = (head // 2) * 128
        raw_key = key_part[:, pair : pair + 128]
        value = values[:, pair : pair + 128]
        if head % 2:
            raw_key = pltpu.roll(raw_key, 64, 1)
            value_first, value_second = pltpu.roll(value, 32, 1), value
        else:
            value_first, value_second = pltpu.roll(value, 96, 1), pltpu.roll(value, 64, 1)
        raw_key = jnp.where(lane < 64, raw_key, rope_part)
        head_query = finish(raw_query, gains[0:1, :])
        head_key = finish(raw_key, gains[1:2, :])
        span = slice(head * rows, (head + 1) * rows)
        out[span, 0:128] = jnp.where(lane < 96, head_query, value_first).astype(jnp.bfloat16)
        out[span, 128:256] = jnp.where(lane < 96, head_key, value_second).astype(jnp.bfloat16)


def attend_kernel(packed, out):
    length = packed.shape[0]
    rows = 256
    scale = 96 ** (-0.5)
    keep = (lane_iota(rows) < 96).astype(jnp.bfloat16)
    query_seg = lax.broadcasted_iota(jnp.int32, (rows, rows), 0) // SPAN
    key_seg = lax.broadcasted_iota(jnp.int32, (rows, rows), 1) // SPAN
    allowed = key_seg <= query_seg
    lane = lane_iota(64)
    for block in range(length // rows):
        first, last = block * rows, (block + 1) * rows
        head_query = packed[first:last, 0:128] * keep
        own = lax.dot_general(
            head_query,
            packed[first:last, 128:256],
            (((1,), (1,)), ((), ())),
            preferred_element_type=jnp.float32,
        )
        own = jnp.where(allowed, own, -1e30)
        top = jnp.max(own, axis=-1, keepdims=True)
        if block:
            past = lax.dot_general(
                head_query,
                packed[0:first, 128:256],
                (((1,), (1,)), ((), ())),
                preferred_element_type=jnp.float32,
            )
            top = jnp.maximum(top, jnp.max(past, axis=-1, keepdims=True))
        raised = jnp.exp((own - top) * scale)
        row_sum = jnp.sum(raised, axis=-1, keepdims=True)
        summed = jnp.dot(
            raised.astype(jnp.bfloat16), packed[first:last, :], preferred_element_type=jnp.float32
        )
        if block:
            raised = jnp.exp((past - top) * scale)
            row_sum = row_sum + jnp.sum(raised, axis=-1, keepdims=True)
            summed = summed + jnp.dot(
                raised.astype(jnp.bfloat16), packed[0:first, :], preferred_element_type=jnp.float32
            )
        summed = summed / row_sum
        for half in range(2):
            low = summed[half * 128 : half * 128 + 64]
            high = summed[half * 128 + 64 : half * 128 + 128]
            joined = jnp.where(
                lane < 64,
                jnp.where(lane < 32, pltpu.roll(low[:, :128], 32, 1), pltpu.roll(low[:, 128:], 64, 1)),
                jnp.where(lane < 96, pltpu.roll(high[:, :128], 96, 1), high[:, 128:]),
            )
            at = (block * 2 + half) * 64
            out[at : at + 64, :] = joined.astype(jnp.bfloat16)


def route_kernel(choice, spread, gather):
    tokens = choice.shape[0]
    experts = lane_iota(tokens)
    first = choice[:, 0:1]
    second = choice[:, 1:2]
    hot_first = (first == experts).astype(jnp.float32)
    hot_second = (second == experts).astype(jnp.float32)
    earlier = (
        lane_iota(tokens) < lax.broadcasted_iota(jnp.int32, (tokens, LANES), 0)
    ).astype(jnp.bfloat16)
    count_first = jnp.dot(
        earlier, hot_first.astype(jnp.bfloat16), preferred_element_type=jnp.float32
    )
    count_second = jnp.dot(
        earlier, hot_second.astype(jnp.bfloat16), preferred_element_type=jnp.float32
    ) + jnp.sum(hot_first, axis=0, keepdims=True)
    rank_first = jnp.sum(count_first * hot_first, axis=-1, keepdims=True).astype(jnp.int32)
    rank_second = jnp.sum(count_second * hot_second, axis=-1, keepdims=True).astype(jnp.int32)
    wide = lane_iota(tokens, 512)
    gather[0:tokens, :] = (first * SLOTS + rank_first == wide).astype(jnp.float32).astype(jnp.bfloat16)
    gather[tokens : 2 * tokens, :] = (
        (second * SLOTS + rank_second == wide).astype(jnp.float32).astype(jnp.bfloat16)
    )
    row_first = jnp.broadcast_to((first * 8 + rank_first).astype(jnp.float32), (tokens, LANES))
    row_second = jnp.broadcast_to((second * 8 + rank_second).astype(jnp.float32), (tokens, LANES))
    row_first = row_first.T[0:1, :].astype(jnp.int32)
    row_second = row_second.T[0:1, :].astype(jnp.int32)
    slot_row = lax.broadcasted_iota(jnp.int32, (spread.shape[0], LANES), 0)
    for half in range(2):
        picked = (slot_row == row_first + 4 * half) | (slot_row == row_second + 4 * half)
        spread[:, half * 128 : half * 128 + 128] = picked.astype(jnp.float32).astype(jnp.bfloat16)


def mix_kernel(
    arrived, residual, mix_gain, out_weight, ffn_gain, spread, stream_out, outgoing, heads_out
):
    tokens = residual.shape[0]
    half_rows = tokens // 2
    lane = lane_iota(half_rows)
    width = residual.shape[1]
    square_low = jnp.zeros((half_rows, 1), jnp.float32)
    square_high = jnp.zeros((half_rows, 1), jnp.float32)
    pairs = arrived.shape[0] // tokens
    for pair in range(pairs):
        one = arrived[pair * tokens : pair * tokens + half_rows, :].astype(jnp.float32)
        two = arrived[pair * tokens + half_rows : (pair + 1) * tokens, :].astype(jnp.float32)
        low = jnp.where(lane < 64, one, pltpu.roll(two, 64, 1))
        high = jnp.where(lane < 64, pltpu.roll(one, 64, 1), two)
        square_low = square_low + jnp.sum(low * low, axis=-1, keepdims=True)
        square_high = square_high + jnp.sum(high * high, axis=-1, keepdims=True)
        heads_out[0:half_rows, pair * 128 : pair * 128 + 128] = low
        heads_out[half_rows:tokens, pair * 128 : pair * 128 + 128] = high
    squares = jnp.concatenate([square_low, square_high], axis=0)
    inverse = lax.rsqrt(squares * (1.0 / heads_out.shape[1]) + eps)
    mixed_in = (heads_out[...] * inverse * mix_gain[...]).astype(jnp.bfloat16)
    stream = residual[...].astype(jnp.float32) + jnp.dot(
        mixed_in, out_weight[...], preferred_element_type=jnp.float32
    )
    stream_out[...] = stream
    normed = (stream * inverse_rms(stream, width) * ffn_gain[...]).astype(jnp.bfloat16)
    stacked = jnp.concatenate([normed[:, : width // 2], normed[:, width // 2 :]], axis=0)
    outgoing[...] = jnp.dot(
        spread[...], stacked, preferred_element_type=jnp.float32
    ).astype(jnp.bfloat16)


def unstack(blocks, rows_out):
    pairs, width = blocks.shape[0] // 16, blocks.shape[1]
    view = blocks[...].astype(jnp.float32).reshape(pairs, 2, 8, width)
    one, two = view[:, 0], view[:, 1]
    upper = lax.broadcasted_iota(jnp.int32, (pairs, 8, width), 1) < 4
    low = jnp.where(upper, one, pltpu.roll(two, 4, 1))
    high = jnp.where(upper, pltpu.roll(one, 4, 1), two)
    rows_out[:, 0:width] = low.reshape(pairs * 8, width).astype(jnp.bfloat16)
    rows_out[:, width : 2 * width] = high.reshape(pairs * 8, width).astype(jnp.bfloat16)


def expert_kernel(arrived, gate_weight, up_weight, down_weight, out, rows_in):
    unstack(arrived, rows_in)
    gate_act = jnp.dot(rows_in[...], gate_weight[0], preferred_element_type=jnp.float32)
    upward = jnp.dot(rows_in[...], up_weight[0], preferred_element_type=jnp.float32)
    hidden = (jax.nn.silu(gate_act) * upward).astype(jnp.bfloat16)
    expert_out = jnp.dot(hidden, down_weight[0], preferred_element_type=jnp.float32)
    rows, width = expert_out.shape
    width = width // 2
    low = expert_out[:, :width].reshape(rows // 8, 8, width)
    high = expert_out[:, width:].reshape(rows // 8, 8, width)
    upper = lax.broadcasted_iota(jnp.int32, (rows // 8, 8, width), 1) < 4
    one = jnp.where(upper, low, pltpu.roll(high, 4, 1))
    two = jnp.where(upper, pltpu.roll(low, 4, 1), high)
    both = jnp.concatenate([one[:, None], two[:, None]], axis=1)
    out[...] = both.reshape(rows * 2, width).astype(jnp.bfloat16)


def combine_kernel(returned, gather, stream, route_weight, out, rows_back):
    unstack(returned, rows_back)
    tokens = stream.shape[0]
    picked = jnp.dot(gather[...], rows_back[...], preferred_element_type=jnp.float32)
    routed = route_weight[:, 0:1] * picked[:tokens] + route_weight[:, 1:2] * picked[tokens:]
    out[...] = (stream[...] + routed).astype(jnp.bfloat16)


def call(body, out_shapes, scratch=(), name=None):
    return pl.pallas_call(
        body,
        out_shape=out_shapes,
        scratch_shapes=list(scratch),
        compiler_params=pltpu.CompilerParams(vmem_limit_bytes=56 * 2**20),
        name=name,
    )


def per_device(
    residual,
    query,
    latent,
    rope_key,
    latent_gain,
    query_gain,
    key_gain,
    key_weight,
    value_weight,
    mix_gain,
    out_weight,
    ffn_gain,
    expert_choice,
    group_prob,
    expert_prob,
    gate_weight,
    up_weight,
    down_weight,
):
    tokens = residual.shape[1]
    width = residual.shape[2]
    sequence = tokens * lax.axis_size("sp")
    shape = jax.ShapeDtypeStruct
    phases = angles(lax.axis_index("sp") * tokens, tokens, rope_key.shape[2])
    cos_table, sin_table = jnp.cos(phases), jnp.sin(phases)
    ones, none = jnp.ones((tokens, 64), jnp.float32), jnp.zeros((tokens, 64), jnp.float32)
    turn = jnp.concatenate(
        [
            ones,
            cos_table,
            cos_table,
            none[:, :32],
            none,
            -sin_table,
            none[:, :48],
            none,
            none[:, :16],
            sin_table,
            none[:, :32],
        ],
        axis=1,
    )
    gains = jnp.pad(jnp.stack([query_gain, key_gain]), ((0, 0), (0, 32)))
    packed = call(project_kernel, shape((16 * tokens, 256), jnp.bfloat16), name="project")(
        query[0],
        latent[0],
        rope_key[0],
        latent_gain[None],
        gains,
        turn,
        key_weight,
        value_weight,
    )
    by_head = lax.all_to_all(packed, "sp", split_axis=0, concat_axis=0, tiled=True)
    spread, gather = call(
        route_kernel,
        (shape((1024, 256), jnp.bfloat16), shape((256, 512), jnp.bfloat16)),
        name="route",
    )(expert_choice[0])
    expert_share = expert_prob[0]
    route_weight = (
        group_prob[0][:, None] * expert_share / jnp.sum(expert_share, axis=-1, keepdims=True)
    )
    head_out = call(attend_kernel, shape((sequence // 2, 128), jnp.bfloat16), name="attend")(by_head)
    by_token = lax.all_to_all(head_out, "sp", split_axis=0, concat_axis=0, tiled=True)
    stream, outgoing = call(
        mix_kernel,
        (shape((tokens, width), jnp.float32), shape((1024, 1024), jnp.bfloat16)),
        scratch=(pltpu.VMEM((tokens, 1024), jnp.float32),),
        name="mix",
    )(by_token, residual[0], mix_gain[None], out_weight, ffn_gain[None], spread)
    arrived = lax.all_to_all(outgoing, ("sp", "dp"), split_axis=0, concat_axis=0, tiled=True)
    answers = call(
        expert_kernel,
        shape((1024, 1024), jnp.bfloat16),
        scratch=(pltpu.VMEM((512, width), jnp.bfloat16),),
        name="expert",
    )(arrived, gate_weight, up_weight, down_weight)
    returned = lax.all_to_all(answers, ("sp", "dp"), split_axis=0, concat_axis=0, tiled=True)
    return call(
        combine_kernel,
        shape((tokens, width), jnp.bfloat16),
        scratch=(pltpu.VMEM((512, width), jnp.bfloat16),),
        name="combine",
    )(returned, gather, stream, route_weight)[None]


def solution(mesh):
    return jax.shard_map(
        per_device,
        mesh=mesh,
        in_specs=(
            P("dp", "sp", None),
            P("dp", "sp", None),
            P("dp", "sp", None),
            P("dp", "sp", None),
            P(),
            P(),
            P(),
            P(),
            P(),
            P(),
            P(),
            P(),
            P("dp", "sp", None),
            P("dp", "sp"),
            P("dp", "sp", None),
            P(("sp", "dp"), None, None),
            P(("sp", "dp"), None, None),
            P(("sp", "dp"), None, None),
        ),
        out_specs=P("dp", "sp", None),
        check_vma=False,
    )
```

time: 181 us -> 149 us (0.82)
  local copies, waits for them, and re-layouts: 41.5 us -> 5.21 us
  Pallas kernels: 0 us -> 34.7 us
  blocking collectives: 38.6 us -> 63.7 us
  matrix products: 20 us -> 0 us
  waiting for transfers between devices: 51 us -> 34 us
  starting transfers between devices: 18.4 us -> 8.07 us
  other arithmetic: 9.68 us -> 2.34 us
    pallas_call x0 -> x6, Pallas kernels: none -> 34.7 us  [the longest x1 8.32 us: per_device(): call(expert_kernel, shape((1024, 1024), jnp.bfloat16), scratch=(pltpu.VME...]
    all_to_all x0 -> x1, blocking collectives: none -> 24.9 us  [per_device(): lax.all_to_all(packed, 'sp', split_axis=0, concat_axis=0, tiled=True)]
    dot_general x13 -> x0, matrix products: 20 us -> none  [the longest x1 5.96 us: per_device(): jnp.dot(hidden, down_weight[0], preferred_element_type=jnp.float32)]
    reshape x6 -> x0, local copies, waits for them, and re-layouts: 18.1 us -> none  [the longest x2 5.71 us: per_device(): returned.reshape(-1, model_width)[target]]
    all_to_all x3 -> x2, waiting for transfers between devices: 51 us -> 34 us  [the longest x1 29.7 us: per_device(): lax.all_to_all(answers, ('sp', 'dp'), split_axis=0, concat_axis=0, tiled=...]
    all_to_all x3 -> x2, starting transfers between devices: 18.4 us -> 8.07 us  [the longest x1 4.54 us: per_device(): lax.all_to_all(answers, ('sp', 'dp'), split_axis=0, concat_axis=0, tiled=...]
    gather x2 -> x0, local copies, waits for them, and re-layouts: 8.51 us -> none  [the longest x1 5.21 us: per_device(): returned.reshape(-1, model_width)[target]]
    unnamed x39 -> x13, local copies, waits for them, and re-layouts: 7.56 us -> 4.3 us
  transfers between devices with their start and end apart: 3 -> 2, of which waited for: 3 -> 2; matrix products, arithmetic and copies ran while one was open for 2% -> 1% of each run, Pallas kernels for 0% -> 2%
where the time goes in v1:
time: 149 us; the launch traced here: 148 us
  blocking collectives  63.7 us (43%)
  Pallas kernels  34.7 us (23%)
  waiting for transfers between devices  34 us (23%)
  starting transfers between devices  8.07 us (5%)
  local copies, waits for them, and re-layouts  5.21 us (3%)
  other arithmetic  2.34 us (2%)
    all_to_all x1, blocking collectives, per_device(): lax.all_to_all(outgoing, ('sp', 'dp'), split_axis=0, concat_axis=0, tiled...  38.8 us
    all_to_all x1, waiting for transfers between devices, per_device(): lax.all_to_all(answers, ('sp', 'dp'), split_axis=0, concat_axis=0, tiled=...  29.7 us
    all_to_all x1, blocking collectives, per_device(): lax.all_to_all(packed, 'sp', split_axis=0, concat_axis=0, tiled=True)  24.9 us
    pallas_call x1, Pallas kernels, per_device(): call(expert_kernel, shape((1024, 1024), jnp.bfloat16), scratch=(pltpu.VME...  8.32 us
    pallas_call x1, Pallas kernels, per_device(): call(project_kernel, shape((16 * tokens, 256), jnp.bfloat16), name='proje...  7.7 us
    pallas_call x1, Pallas kernels, per_device(): call(attend_kernel, shape((sequence // 2, 128), jnp.bfloat16), name='atte...  6.8 us
    pallas_call x1, Pallas kernels, per_device(): call(mix_kernel, (shape((tokens, width), jnp.float32), shape((1024, 1024)...  5.78 us
    all_to_all x1, starting transfers between devices, per_device(): lax.all_to_all(answers, ('sp', 'dp'), split_axis=0, concat_axis=0, tiled=...  4.54 us
  transfers between devices with their start and end apart: 2, of which 2 were waited for; matrix products, arithmetic and copies ran while one was open for 1% of the time, Pallas kernels for 2%

profile of v1, /device:TPU:1, one launch (start us, length us, event | category | flops | bytes accessed | tf_op | source)
XLA Modules:
  0.0 148.2 jit_solution(8432998299745017749)
XLA Ops:
  0.0 1.4 copy.22
  1.4 0.3 multiply_sine_fusion
  1.7 1.3 select_maximum_fusion.gains
  3.1 0.9 concatenate.3.turn
  4.0 7.7 %project.1 = bf16[2048,256]{1,0:T(8,128)(2,1)} custom-call(bf16[128,1536]{1,0:T(8,128)(2,1)} %bitcast.33, bf16[128,256]{1,0:T(8,128)(2,1)} %bitcast.36, bf16[128,32]{1,0:T(8,128)(2,1)} %bitcast.35, f32[1,256]{1,0:T(1,128)} %bitcast.39, f32[2,128]{1,0:T(2,128)} %select_maximum_fusion.gains, f32[128,384]{1,0:T(8,128)} %concatenate.3.turn, ...), custom_call_target="tpu_custom_call" | custom-call | tf_op jit(solution)/shard_map/project/pallas_call | solution.py:293
  11.7 24.9 %all_to_all.44 = bf16[16,128,256]{2,1,0:T(8,128)(2,1)} all-to-all(bf16[16,128,256]{2,1,0:T(8,128)(2,1)} %bitcast.28), channel_id=1, replica_groups=mesh['sp'=16,'dp'=8] {'sp'}, dimensions={0} | all-to-all | bytes 2097152 | tf_op jit(solution)/shard_map/all_to_all | solution.py:303
  36.5 6.8 %attend.1 = bf16[1024,128]{1,0:T(8,128)(2,1)} custom-call(bf16[2048,256]{1,0:T(8,128)(2,1)} %bitcast.27), custom_call_target="tpu_custom_call" | custom-call | tf_op jit(solution)/shard_map/attend/pallas_call | solution.py:313
  43.3 3.5 %all-to-all-start.1 = ((bf16[16,64,128]{2,1,0:T(8,128)(2,1)}), bf16[16,64,128]{2,1,0:T(8,128)(2,1)S(1)}, u32[]{:S(2)}, u32[]{:S(2)}) async-start(bf16[16,64,128]{2,1,0:T(8,128)(2,1)} %bitcast.31), calls=%async_computation.1 | async-start | bytes 524288 | tf_op jit(solution)/shard_map/all_to_all | solution.py:314
  46.9 0.0 copy-done.3
  46.9 0.7 copy.24
  47.6 2.4 %route.1 = (bf16[1024,256]{1,0:T(8,128)(2,1)}, bf16[256,512]{1,0:T(8,128)(2,1)}) custom-call(s32[128,2]{1,0:T(8,128)} %bitcast.34), custom_call_target="tpu_custom_call" | custom-call | tf_op jit(solution)/shard_map/route/pallas_call | solution.py:304
  50.0 4.3 %all-to-all-done.1 = bf16[16,64,128]{2,1,0:T(8,128)(2,1)S(1)} async-done(((bf16[16,64,128]{2,1,0:T(8,128)(2,1)}), bf16[16,64,128]{2,1,0:T(8,128)(2,1)S(1)}, u32[]{:S(2)}, u32[]{:S(2)}) %all-to-all-start.1) | async-done | bytes 262176 | tf_op jit(solution)/shard_map/all_to_all | solution.py:314
  54.4 0.7 copy-done.1
  55.1 5.8 %mix.1 = (f32[128,2048]{1,0:T(8,128)}, bf16[1024,1024]{1,0:T(8,128)(2,1)}) custom-call(bf16[1024,128]{1,0:T(8,128)(2,1)} %bitcast.30, bf16[128,2048]{1,0:T(8,128)(2,1)} %bitcast.32, f32[1,1024]{1,0:T(1,128)} %bitcast.38, bf16[1024,2048]{1,0:T(8,128)(2,1)} %out_weight.1, f32[1,2048]{1,0:T(1,128)} %bitcast.37, bf16[1024,256]{1,0:T(8,128)(2,1)} %get-tuple-element.9.spread), custom_call_target="tpu_custom_call" | custom-call | tf_op jit(solution)/shard_map/mix/pallas_call | solution.py:315
  60.8 38.8 %all_to_all.45 = bf16[128,8,1024]{2,1,0:T(8,128)(2,1)} all-to-all(bf16[128,8,1024]{2,1,0:T(8,128)(2,1)} %bitcast.29), channel_id=1, replica_groups=mesh['sp'=16,'dp'=8] {'sp','dp'}, dimensions={0} | all-to-all | bytes 4194304 | tf_op jit(solution)/shard_map/all_to_all | solution.py:321
  99.7 8.3 %expert.1 = bf16[1024,1024]{1,0:T(8,128)(2,1)} custom-call(bf16[1024,1024]{1,0:T(8,128)(2,1)} %bitcast.25, bf16[1,2048,512]{2,1,0:T(8,128)(2,1)} %gate_weight.1, bf16[1,2048,512]{2,1,0:T(8,128)(2,1)} %up_weight.1, bf16[1,512,2048]{2,1,0:T(8,128)(2,1)} %down_weight.1), custom_call_target="tpu_custom_call" | custom-call | tf_op jit(solution)/shard_map/expert/pallas_call | solution.py:322
  108.0 4.5 %all-to-all-start.3 = ((bf16[128,8,1024]{2,1,0:T(8,128)(2,1)}), bf16[128,8,1024]{2,1,0:T(8,128)(2,1)S(1)}, u32[]{:S(2)}, u32[]{:S(2)}) async-start(bf16[128,8,1024]{2,1,0:T(8,128)(2,1)} %bitcast.24), calls=%async_computation.3 | async-start | bytes 4194304 | tf_op jit(solution)/shard_map/all_to_all | solution.py:328
  112.6 0.0 copy-done.2
  112.6 0.1 copy.25
  112.7 0.0 copy-done.4
  112.7 0.7 fusion.route_weight
  113.4 29.7 %all-to-all-done.3 = bf16[128,8,1024]{2,1,0:T(8,128)(2,1)S(1)} async-done(((bf16[128,8,1024]{2,1,0:T(8,128)(2,1)}), bf16[128,8,1024]{2,1,0:T(8,128)(2,1)S(1)}, u32[]{:S(2)}, u32[]{:S(2)}) %all-to-all-start.3) | async-done | bytes 2097184 | tf_op jit(solution)/shard_map/all_to_all | solution.py:328
  143.2 1.3 copy-done
  144.5 3.7 %combine.1 = bf16[128,2048]{1,0:T(8,128)(2,1)} custom-call(bf16[1024,1024]{1,0:T(8,128)(2,1)} %bitcast.26, bf16[256,512]{1,0:T(8,128)(2,1)} %get-tuple-element.11.gather, f32[128,2048]{1,0:T(8,128)} %get-tuple-element.12.stream, f32[128,2]{1,0:T(8,128)} %fusion.route_weight), custom_call_target="tpu_custom_call" | custom-call | tf_op jit(solution)/shard_map/combine/pallas_call | solution.py:329
  (13 shorter events, 0.1 us)
Async XLA Ops:
  11.7 35.2 %copy-start.3 = (s32[1,128,2]{1,2,0:T(2,128)S(1)}, s32[1,128,2]{1,2,0:T(2,128)}, u32[]{:S(2)}) copy-start(s32[1,128,2]{1,2,0:T(2,128)} %param.30) | copy-start | bytes 3076
  43.3 11.0 %all-to-all-start.1 = ((bf16[16,64,128]{2,1,0:T(8,128)(2,1)}), bf16[16,64,128]{2,1,0:T(8,128)(2,1)S(1)}, u32[]{:S(2)}, u32[]{:S(2)}) async-start(bf16[16,64,128]{2,1,0:T(8,128)(2,1)} %bitcast.31), calls=%async_computation.1 | async-start | bytes 524288 | tf_op jit(solution)/shard_map/all_to_all | solution.py:314
  54.4 0.7 copy-start.1
  108.0 4.6 %copy-start.2 = (f32[1,128,2]{1,2,0:T(2,128)S(1)}, f32[1,128,2]{1,2,0:T(2,128)}, u32[]{:S(2)}) copy-start(f32[1,128,2]{1,2,0:T(2,128)} %param.32) | copy-start | bytes 3076
  108.0 4.7 %copy-start.4 = (f32[1,128]{1,0:T(1,128)S(1)}, f32[1,128]{1,0:T(1,128)}, u32[]{:S(2)}) copy-start(f32[1,128]{1,0:T(1,128)} %param.31) | copy-start | bytes 1540
  108.0 35.2 %all-to-all-start.3 = ((bf16[128,8,1024]{2,1,0:T(8,128)(2,1)}), bf16[128,8,1024]{2,1,0:T(8,128)(2,1)S(1)}, u32[]{:S(2)}, u32[]{:S(2)}) async-start(bf16[128,8,1024]{2,1,0:T(8,128)(2,1)} %bitcast.24), calls=%async_computation.3 | async-start | bytes 4194304 | tf_op jit(solution)/shard_map/all_to_all | solution.py:328
  143.2 1.3 copy-start

commit v2 on v1

v2 whole, which is shorter than its diff:
```python
import jax
import jax.numpy as jnp
from jax import lax
from jax.experimental import pallas as pl
from jax.experimental.pallas import tpu as pltpu
from jax.sharding import PartitionSpec as P

SPAN = 64
LANES = 128
SLOTS = 4

eps = 1e-06


def angles(offset, span_count, rope_width):
    position = (offset + jnp.arange(span_count, dtype=jnp.int32)).astype(jnp.float32)
    frequency = 10000.0 ** (-2.0 * jnp.arange(rope_width // 2, dtype=jnp.float32) / rope_width)
    return position[:, None] * frequency[None, :]


def lane_iota(rows, width=LANES):
    return lax.broadcasted_iota(jnp.int32, (rows, width), 1)


def inverse_rms(vector, width):
    return lax.rsqrt(jnp.sum(vector * vector, axis=-1, keepdims=True) * (1.0 / width) + eps)


def turn_lanes(vector, cos_part, minus_sin, plus_sin):
    return (
        vector * cos_part
        + pltpu.roll(vector, 112, 1) * minus_sin
        + pltpu.roll(vector, 16, 1) * plus_sin
    )


def split_high_low(vector):
    high = vector.astype(jnp.bfloat16)
    low = (vector - high.astype(jnp.float32)).astype(jnp.bfloat16)
    return jnp.concatenate([high, low], axis=1)


def same_group(group_of_row, group_of_lane):
    ones = (group_of_row == group_of_lane).astype(jnp.float32).astype(jnp.bfloat16)
    return jnp.concatenate([ones, ones], axis=0)


def project_kernel(
    query,
    latent,
    rope,
    latent_gain,
    query_gain,
    key_gain,
    cos_table,
    sin_table,
    key_weight,
    value_weight,
    out,
    small,
    turn,
):
    rows = query.shape[0]
    heads = query.shape[1] // 96
    lane = lane_iota(rows)
    raw_latent = latent[...].astype(jnp.float32)
    normed_latent = (
        raw_latent * inverse_rms(raw_latent, raw_latent.shape[1]) * latent_gain[...]
    ).astype(jnp.bfloat16)
    key_part = (
        jnp.dot(normed_latent, key_weight[...], preferred_element_type=jnp.float32)
        .astype(jnp.bfloat16)
        .astype(jnp.float32)
    )
    values = jnp.dot(normed_latent, value_weight[...], preferred_element_type=jnp.float32)

    small[...] = jnp.zeros(small.shape, jnp.float32)
    small[0:1, 0:96] = query_gain[...]
    small[8:9, 0:96] = key_gain[...]
    turn[:, 0:128] = jnp.ones((rows, 128), jnp.float32)
    turn[:, 128:384] = jnp.zeros((rows, 256), jnp.float32)
    turn[:, 64:80] = cos_table[...]
    turn[:, 80:96] = cos_table[...]
    turn[:, 192:208] = -sin_table[...]
    turn[:, 336:352] = sin_table[...]
    tables = [turn[:, 0:128], turn[:, 128:256], turn[:, 256:384]]
    gain_row = small[0:8, :]
    key_gain_row = small[8:9, :]
    gain_tiles = [
        (gain_row + pltpu.roll(gain_row, 96, 1) * (lane_iota(8) >= 96).astype(jnp.float32))[0:1],
        jnp.where(lane_iota(8) < 64, pltpu.roll(gain_row, 96, 1), pltpu.roll(gain_row, 64, 1))[0:1],
        jnp.where(lane_iota(8) < 32, pltpu.roll(gain_row, 64, 1), pltpu.roll(gain_row, 32, 1))[0:1],
    ]
    turn_tiles = [
        tables,
        [pltpu.roll(t, 96, 1) for t in tables],
        [jnp.where(lane < 64, pltpu.roll(t, 64, 1), pltpu.roll(t, 32, 1)) for t in tables],
    ]
    wide_row = lax.broadcasted_iota(jnp.int32, (128, 256), 0)
    wide_lane = lax.broadcasted_iota(jnp.int32, (128, 256), 1)
    sum_low = same_group(wide_row // 96, wide_lane // 96)
    sum_mid = same_group((wide_row + 128) // 96, wide_lane // 96)
    sum_mid_last = same_group(
        (lax.broadcasted_iota(jnp.int32, (128, 128), 0) + 128) // 96, (lane_iota(128) + 256) // 96
    )
    sum_high = same_group((wide_row + 256) // 96, (wide_lane + 128) // 96)
    sum_pair = same_group(
        lax.broadcasted_iota(jnp.int32, (128, 128), 0) // 64, lane_iota(128) // 64
    )
    sum_all = jnp.ones((256, 128), jnp.bfloat16)

    place = (
        lax.broadcasted_iota(jnp.int32, (32, LANES), 0) + 64 == lane_iota(32)
    ).astype(jnp.float32).astype(jnp.bfloat16)
    rope_part = lax.dot_general(
        rope[...], place, (((0,), (0,)), ((), ())), preferred_element_type=jnp.float32
    )
    rope_square = jnp.dot(
        split_high_low(rope_part * rope_part), sum_all, preferred_element_type=jnp.float32
    )
    rope_turned = turn_lanes(rope_part * key_gain_row, *tables)
    rope_at = [rope_turned] + [pltpu.roll(rope_turned, shift, 1) for shift in (96, 64, 32)]
    low_gain = jnp.where(lane_iota(8) < 64, small[8:16, :], pltpu.roll(small[8:16, :], 64, 1))[0:1]

    for four in range(heads // 4):
        raw = [
            query[:, four * 384 + t * 128 : four * 384 + t * 128 + 128].astype(jnp.float32)
            for t in range(3)
        ]
        squares = [split_high_low(t * t) for t in raw]
        from_low = jnp.dot(squares[0], sum_low, preferred_element_type=jnp.float32)
        from_mid = jnp.dot(squares[1], sum_mid, preferred_element_type=jnp.float32)
        from_mid_last = jnp.dot(squares[1], sum_mid_last, preferred_element_type=jnp.float32)
        from_high = jnp.dot(squares[2], sum_high, preferred_element_type=jnp.float32)
        sums = [
            from_low[:, :128] + from_mid[:, :128],
            from_low[:, 128:] + from_mid[:, 128:] + from_high[:, :128],
            from_mid_last + from_high[:, 128:],
        ]
        turned = [
            turn_lanes(
                raw[t] * lax.rsqrt(sums[t] * (1.0 / 96) + eps) * gain_tiles[t], *turn_tiles[t]
            )
            for t in range(3)
        ]
        query_at = [
            turned[0],
            jnp.where(lane < 96, turned[1], turned[0]),
            jnp.where(lane < 64, turned[2], turned[1]),
            turned[2],
        ]
        for pair in range(2):
            at = (four * 2 + pair) * 128
            part = key_part[:, at : at + 128]
            value = values[:, at : at + 128]
            sums = (
                jnp.dot(split_high_low(part * part), sum_pair, preferred_element_type=jnp.float32)
                + rope_square
            )
            inverse = lax.rsqrt(sums * (1.0 / 96) + eps)
            part = part * low_gain * inverse
            if pair == 0:
                inverse = pltpu.roll(inverse, 64, 1)
                keys = [
                    jnp.where(lane < 64, part, rope_at[0] * inverse),
                    jnp.where(
                        (lane >= 32) & (lane < 64), rope_at[1] * inverse, pltpu.roll(part, 32, 1)
                    ),
                ]
                value_first = [pltpu.roll(value, 96, 1), value]
                value_second = [pltpu.roll(value, 64, 1), pltpu.roll(value, 96, 1)]
                free = [lane >= 96, (lane >= 64) & (lane < 96)]
            else:
                keys = [
                    jnp.where(lane < 64, rope_at[2] * inverse, pltpu.roll(part, 64, 1)),
                    jnp.where(lane >= 96, rope_at[3] * inverse, pltpu.roll(part, 96, 1)),
                ]
                value_first = [pltpu.roll(value, 32, 1), pltpu.roll(value, 64, 1)]
                value_second = [value, pltpu.roll(value, 32, 1)]
                free = [(lane >= 32) & (lane < 64), lane < 32]
            for odd in range(2):
                head = four * 4 + pair * 2 + odd
                span = slice(head * rows, (head + 1) * rows)
                head_query = query_at[pair * 2 + odd]
                out[span, 0:128] = jnp.where(free[odd], value_first[odd], head_query).astype(
                    jnp.bfloat16
                )
                out[span, 128:256] = jnp.where(free[odd], value_second[odd], keys[odd]).astype(
                    jnp.bfloat16
                )


def attend_kernel(start, packed, out):
    length = packed.shape[0]
    rows = 256
    scale = 96 ** (-0.5)
    begin = start[0]
    keep = (((lane_iota(16) - begin + 128) % 128) < 96).astype(jnp.float32).astype(jnp.bfloat16)[0:1]
    query_seg = lax.broadcasted_iota(jnp.int32, (rows, rows), 0) // SPAN
    key_seg = lax.broadcasted_iota(jnp.int32, (rows, rows), 1) // SPAN
    allowed = key_seg <= query_seg
    lane = lane_iota(64)
    to_front = (160 - begin) % 128

    def fold(array, combine):
        parts = [array[:, at : at + 128] for at in range(0, array.shape[1], 128)]
        while len(parts) > 1:
            parts = [combine(*parts[at : at + 2]) if at + 1 < len(parts) else parts[at] for at in range(0, len(parts), 2)]
        return parts[0]

    for block in range(length // rows):
        first, last = block * rows, (block + 1) * rows
        head_query = packed[first:last, 0:128] * keep
        scores = lax.dot_general(
            head_query,
            packed[0:last, 128:256],
            (((1,), (1,)), ((), ())),
            preferred_element_type=jnp.float32,
        )
        own = jnp.where(allowed, scores[:, first:last], -1e30)
        if block:
            scores = jnp.concatenate([scores[:, :first], own], axis=1)
        else:
            scores = own
        top = jnp.max(fold(scores, jnp.maximum), axis=-1, keepdims=True)
        raised = jnp.exp((scores - top) * scale)
        row_sum = jnp.sum(fold(raised, jnp.add), axis=-1, keepdims=True)
        summed = jnp.dot(
            raised.astype(jnp.bfloat16), packed[0:last, :], preferred_element_type=jnp.float32
        )
        summed = summed * (1.0 / row_sum)
        for half in range(2):
            low = summed[half * 128 : half * 128 + 64]
            high = summed[half * 128 + 64 : half * 128 + 128]
            joined = jnp.where(
                lane < 64,
                jnp.where(
                    lane < 32,
                    pltpu.roll(low[:, :128], to_front, 1),
                    pltpu.roll(low[:, 128:], (to_front + 32) % 128, 1),
                ),
                jnp.where(
                    lane < 96,
                    pltpu.roll(high[:, :128], (to_front + 64) % 128, 1),
                    pltpu.roll(high[:, 128:], (to_front + 96) % 128, 1),
                ),
            )
            at = (block * 2 + half) * 64
            out[at : at + 64, :] = joined.astype(jnp.bfloat16)


def route_kernel(choice, group_prob, shares, spread, gather, weight):
    tokens = choice.shape[1]
    expert = lax.broadcasted_iota(jnp.int32, (LANES, tokens), 0)
    first = choice[0:1, :]
    second = choice[1:2, :]
    hot_first = (expert == first).astype(jnp.float32)
    hot_second = (expert == second).astype(jnp.float32)
    earlier = (
        (lax.broadcasted_iota(jnp.int32, (tokens, tokens), 0) < lane_iota(tokens, tokens))
        .astype(jnp.float32)
        .astype(jnp.bfloat16)
    )
    count_first = jnp.dot(
        hot_first.astype(jnp.bfloat16), earlier, preferred_element_type=jnp.float32
    )
    count_second = jnp.dot(
        hot_second.astype(jnp.bfloat16), earlier, preferred_element_type=jnp.float32
    ) + jnp.sum(hot_first, axis=1, keepdims=True)
    rank_first = jnp.sum(count_first * hot_first, axis=0, keepdims=True).astype(jnp.int32)
    rank_second = jnp.sum(count_second * hot_second, axis=0, keepdims=True).astype(jnp.int32)
    row_first = first * 8 + rank_first
    row_second = second * 8 + rank_second
    slot_row = lax.broadcasted_iota(jnp.int32, (spread.shape[0], tokens), 0)
    for half in range(2):
        picked = (slot_row == row_first + 4 * half) | (slot_row == row_second + 4 * half)
        spread[:, half * 128 : half * 128 + 128] = picked.astype(jnp.float32).astype(jnp.bfloat16)
    wide = lane_iota(tokens, 512)

    def down(row):
        return jnp.broadcast_to(row.astype(jnp.float32), (tokens, tokens)).T[:, 0:1]

    for k, (chosen, rank) in enumerate(((first, rank_first), (second, rank_second))):
        target = down(chosen * SLOTS + rank).astype(jnp.int32)
        gather[k * tokens : (k + 1) * tokens, :] = (
            (target == wide).astype(jnp.float32).astype(jnp.bfloat16)
        )
    total = shares[0:1, :] + shares[1:2, :]
    weight[:, 0:1] = down(group_prob[...] * shares[0:1, :] / total)
    weight[:, 1:2] = down(group_prob[...] * shares[1:2, :] / total)


def mix_kernel(
    arrived, residual, mix_gain, out_weight, ffn_gain, spread, stream_out, outgoing, heads_out
):
    tokens = residual.shape[0]
    half_rows = tokens // 2
    lane = lane_iota(half_rows)
    width = residual.shape[1]
    square_low = jnp.zeros((half_rows, 1), jnp.float32)
    square_high = jnp.zeros((half_rows, 1), jnp.float32)
    pairs = arrived.shape[0] // tokens
    for pair in range(pairs):
        one = arrived[pair * tokens : pair * tokens + half_rows, :].astype(jnp.float32)
        two = arrived[pair * tokens + half_rows : (pair + 1) * tokens, :].astype(jnp.float32)
        low = jnp.where(lane < 64, one, pltpu.roll(two, 64, 1))
        high = jnp.where(lane < 64, pltpu.roll(one, 64, 1), two)
        square_low = square_low + jnp.sum(low * low, axis=-1, keepdims=True)
        square_high = square_high + jnp.sum(high * high, axis=-1, keepdims=True)
        heads_out[0:half_rows, pair * 128 : pair * 128 + 128] = low
        heads_out[half_rows:tokens, pair * 128 : pair * 128 + 128] = high
    squares = jnp.concatenate([square_low, square_high], axis=0)
    inverse = lax.rsqrt(squares * (1.0 / heads_out.shape[1]) + eps)
    mixed_in = (heads_out[...] * inverse * mix_gain[...]).astype(jnp.bfloat16)
    stream = residual[...].astype(jnp.float32) + jnp.dot(
        mixed_in, out_weight[...], preferred_element_type=jnp.float32
    )
    stream_out[...] = stream
    normed = (stream * inverse_rms(stream, width) * ffn_gain[...]).astype(jnp.bfloat16)
    stacked = jnp.concatenate([normed[:, : width // 2], normed[:, width // 2 :]], axis=0)
    outgoing[...] = jnp.dot(
        spread[...], stacked, preferred_element_type=jnp.float32
    ).astype(jnp.bfloat16)


def unstack(blocks, rows_out):
    pairs, width = blocks.shape[0] // 16, blocks.shape[1]
    view = blocks[...].astype(jnp.float32).reshape(pairs, 2, 8, width)
    one, two = view[:, 0], view[:, 1]
    upper = lax.broadcasted_iota(jnp.int32, (pairs, 8, width), 1) < 4
    low = jnp.where(upper, one, pltpu.roll(two, 4, 1))
    high = jnp.where(upper, pltpu.roll(one, 4, 1), two)
    rows_out[:, 0:width] = low.reshape(pairs * 8, width).astype(jnp.bfloat16)
    rows_out[:, width : 2 * width] = high.reshape(pairs * 8, width).astype(jnp.bfloat16)


def expert_kernel(arrived, gate_weight, up_weight, down_weight, out, rows_in):
    unstack(arrived, rows_in)
    gate_act = jnp.dot(rows_in[...], gate_weight[0], preferred_element_type=jnp.float32)
    upward = jnp.dot(rows_in[...], up_weight[0], preferred_element_type=jnp.float32)
    hidden = (jax.nn.silu(gate_act) * upward).astype(jnp.bfloat16)
    expert_out = jnp.dot(hidden, down_weight[0], preferred_element_type=jnp.float32)
    rows, width = expert_out.shape
    width = width // 2
    low = expert_out[:, :width].reshape(rows // 8, 8, width)
    high = expert_out[:, width:].reshape(rows // 8, 8, width)
    upper = lax.broadcasted_iota(jnp.int32, (rows // 8, 8, width), 1) < 4
    one = jnp.where(upper, low, pltpu.roll(high, 4, 1))
    two = jnp.where(upper, pltpu.roll(low, 4, 1), high)
    both = jnp.concatenate([one[:, None], two[:, None]], axis=1)
    out[...] = both.reshape(rows * 2, width).astype(jnp.bfloat16)


def combine_kernel(returned, gather, stream, route_weight, out, rows_back):
    unstack(returned, rows_back)
    tokens = stream.shape[0]
    picked = jnp.dot(gather[...], rows_back[...], preferred_element_type=jnp.float32)
    routed = route_weight[:, 0:1] * picked[:tokens] + route_weight[:, 1:2] * picked[tokens:]
    out[...] = (stream[...] + routed).astype(jnp.bfloat16)


def call(body, out_shapes, mib, scratch=(), name=None, scalars=0):
    spec = [pl.BlockSpec(memory_space=pltpu.SMEM)] * scalars
    extra = {}

    def run(*operands):
        if scalars:
            extra["in_specs"] = spec + [
                pl.BlockSpec(memory_space=pltpu.VMEM) for _ in operands[scalars:]
            ]
        return pl.pallas_call(
            body,
            out_shape=out_shapes,
            scratch_shapes=list(scratch),
            compiler_params=pltpu.CompilerParams(vmem_limit_bytes=mib * 2**20),
            name=name,
            **extra,
        )(*operands)

    return run


def per_device(
    residual,
    query,
    latent,
    rope_key,
    latent_gain,
    query_gain,
    key_gain,
    key_weight,
    value_weight,
    mix_gain,
    out_weight,
    ffn_gain,
    expert_choice,
    group_prob,
    expert_prob,
    gate_weight,
    up_weight,
    down_weight,
):
    tokens = residual.shape[1]
    width = residual.shape[2]
    sequence = tokens * lax.axis_size("sp")
    shape = jax.ShapeDtypeStruct
    phases = angles(lax.axis_index("sp") * tokens, tokens, rope_key.shape[2])
    packed = call(
        project_kernel,
        shape((16 * tokens, 256), jnp.bfloat16),
        12,
        scratch=(pltpu.VMEM((16, 128), jnp.float32), pltpu.VMEM((tokens, 384), jnp.float32)),
        name="project",
    )(
        query[0],
        latent[0],
        rope_key[0].T,
        latent_gain[None],
        query_gain[None],
        key_gain[None],
        jnp.cos(phases),
        jnp.sin(phases),
        key_weight,
        value_weight,
    )
    by_head = lax.all_to_all(packed, "sp", split_axis=0, concat_axis=0, tiled=True)
    spread, gather, route_weight = call(
        route_kernel,
        (
            shape((1024, 256), jnp.bfloat16),
            shape((256, 512), jnp.bfloat16),
            shape((tokens, 2), jnp.float32),
        ),
        8,
        name="route",
    )(expert_choice[0].T, group_prob, expert_prob[0].T)
    start = (lax.axis_index("sp") * 96) % 128
    head_out = call(
        attend_kernel, shape((sequence // 2, 128), jnp.bfloat16), 20, name="attend", scalars=1
    )(start[None].astype(jnp.int32), by_head)
    by_token = lax.all_to_all(head_out, "sp", split_axis=0, concat_axis=0, tiled=True)
    stream, outgoing = call(
        mix_kernel,
        (shape((tokens, width), jnp.float32), shape((1024, 1024), jnp.bfloat16)),
        16,
        scratch=(pltpu.VMEM((tokens, 1024), jnp.float32),),
        name="mix",
    )(by_token, residual[0], mix_gain[None], out_weight, ffn_gain[None], spread)
    arrived = lax.all_to_all(outgoing, ("sp", "dp"), split_axis=0, concat_axis=0, tiled=True)
    answers = call(
        expert_kernel,
        shape((1024, 1024), jnp.bfloat16),
        20,
        scratch=(pltpu.VMEM((512, width), jnp.bfloat16),),
        name="expert",
    )(arrived, gate_weight, up_weight, down_weight)
    returned = lax.all_to_all(answers, ("sp", "dp"), split_axis=0, concat_axis=0, tiled=True)
    return call(
        combine_kernel,
        shape((tokens, width), jnp.bfloat16),
        14,
        scratch=(pltpu.VMEM((512, width), jnp.bfloat16),),
        name="combine",
    )(returned, gather, stream, route_weight)[None]


def solution(mesh):
    return jax.shard_map(
        per_device,
        mesh=mesh,
        in_specs=(
            P("dp", "sp", None),
            P("dp", "sp", None),
            P("dp", "sp", None),
            P("dp", "sp", None),
            P(),
            P(),
            P(),
            P(),
            P(),
            P(),
            P(),
            P(),
            P("dp", "sp", None),
            P("dp", "sp"),
            P("dp", "sp", None),
            P(("sp", "dp"), None, None),
            P(("sp", "dp"), None, None),
            P(("sp", "dp"), None, None),
        ),
        out_specs=P("dp", "sp", None),
        check_vma=False,
    )
```

time: 149 us -> 134 us (0.90)
  Pallas kernels: 34.7 us -> 15.9 us
  waiting for transfers between devices: 34 us -> 23 us
  blocking collectives: 63.7 us -> 72.6 us
  starting transfers between devices: 8.07 us -> 12.9 us
  local copies, waits for them, and re-layouts: 5.21 us -> 8.82 us
  other arithmetic: 2.34 us -> 0.32 us
    pallas_call x6, Pallas kernels: 34.7 us -> 15.9 us  [run(): pl.pallas_call(body, out_shape=out_shapes, scratch_shapes=list(scratch),...]
    all_to_all x1, waiting for transfers between devices: 29.7 us -> 16 us  [per_device(): lax.all_to_all(packed, 'sp', split_axis=0, concat_axis=0, tiled=True)]
    all_to_all x1, blocking collectives: 24.9 us -> 34.4 us  [per_device(): lax.all_to_all(answers, ('sp', 'dp'), split_axis=0, concat_axis=0, tiled=...]
    unnamed x13 -> x36, local copies, waits for them, and re-layouts: 4.3 us -> 8.82 us
    all_to_all x1, starting transfers between devices: 4.54 us -> 8.73 us  [per_device(): lax.all_to_all(packed, 'sp', split_axis=0, concat_axis=0, tiled=True)]
    all_to_all x1, waiting for transfers between devices: 4.32 us -> 7.01 us  [per_device(): lax.all_to_all(head_out, 'sp', split_axis=0, concat_axis=0, tiled=True)]
  transfers between devices with their start and end apart: 2 -> 2, of which waited for: 2 -> 2; matrix products, arithmetic and copies ran while one was open for 1% -> 0% of each run, Pallas kernels for 2% -> 0%
where the time goes in v2:
time: 134 us
  blocking collectives  72.6 us (54%)
  waiting for transfers between devices  23 us (17%)
  Pallas kernels  15.9 us (12%)
  starting transfers between devices  12.9 us (10%)
  local copies, waits for them, and re-layouts  8.82 us (7%)
    all_to_all x1, blocking collectives, per_device(): lax.all_to_all(outgoing, ('sp', 'dp'), split_axis=0, concat_axis=0, tiled...  38.3 us
    all_to_all x1, blocking collectives, per_device(): lax.all_to_all(answers, ('sp', 'dp'), split_axis=0, concat_axis=0, tiled=...  34.4 us
    all_to_all x1, waiting for transfers between devices, per_device(): lax.all_to_all(packed, 'sp', split_axis=0, concat_axis=0, tiled=True)  16 us
    pallas_call x6, Pallas kernels, run(): pl.pallas_call(body, out_shape=out_shapes, scratch_shapes=list(scratch),...  15.9 us
    unnamed x36, local copies, waits for them, and re-layouts  8.82 us
    all_to_all x1, starting transfers between devices, per_device(): lax.all_to_all(packed, 'sp', split_axis=0, concat_axis=0, tiled=True)  8.73 us
    all_to_all x1, waiting for transfers between devices, per_device(): lax.all_to_all(head_out, 'sp', split_axis=0, concat_axis=0, tiled=True)  7.01 us
    all_to_all x1, starting transfers between devices, per_device(): lax.all_to_all(head_out, 'sp', split_axis=0, concat_axis=0, tiled=True)  4.2 us
  transfers between devices with their start and end apart: 2, of which 2 were waited for; matrix products, arithmetic and copies ran while one was open for 0% of the time, Pallas kernels for 0%

profile of v2, /device:TPU:1, one launch (start us, length us, event | category | flops | bytes accessed | tf_op | source)
XLA Modules:
  0.0 133.8 jit_solution(9110192652690420531)
XLA Ops:
  0.0 0.3 multiply_sine_fusion
  0.4 1.0 copy-done.5
  1.4 1.0 copy-done.6
  2.4 1.0 copy-done.7
  3.4 0.8 copy-done.8
  4.3 0.7 copy-done.9
  5.0 0.7 copy-done.12
  5.6 0.7 copy-done.15
  6.3 0.7 copy-done.16
  7.0 2.7 %project.1 = bf16[2048,256]{1,0:T(8,128)(2,1)} custom-call(bf16[128,1536]{1,0:T(8,128)(2,1)S(1)} %bitcast.34, bf16[128,256]{1,0:T(8,128)(2,1)S(1)} %bitcast.35, bf16[32,128]{1,0:T(8,128)(2,1)S(1)} %bitcast.36, f32[1,256]{1,0:T(1,128)S(1)} %bitcast.39, f32[1,96]{1,0:T(1,128)S(1)} %bitcast.42, f32[1,96]{1,0:T(1,128)S(1)} %bitcast.43, ...), custom_call_target="tpu_custom_call" | custom-call | tf_op jit(solution)/shard_map/project/pallas_call | solution.py:371
  9.6 0.0 copy-start.10
  9.6 8.7 %all-to-all-start = ((bf16[16,128,256]{2,1,0:T(8,128)(2,1)}), bf16[16,128,256]{2,1,0:T(8,128)(2,1)S(1)}, u32[]{:S(2)}, u32[]{:S(2)}) async-start(bf16[16,128,256]{2,1,0:T(8,128)(2,1)} %bitcast.8), calls=%async_computation | async-start | bytes 2097152 | tf_op jit(solution)/shard_map/all_to_all | solution.py:426
  18.4 16.0 %all-to-all-done = bf16[16,128,256]{2,1,0:T(8,128)(2,1)S(1)} async-done(((bf16[16,128,256]{2,1,0:T(8,128)(2,1)}), bf16[16,128,256]{2,1,0:T(8,128)(2,1)S(1)}, u32[]{:S(2)}, u32[]{:S(2)}) %all-to-all-start) | async-done | bytes 1048608 | tf_op jit(solution)/shard_map/all_to_all | solution.py:426
  34.4 5.5 %attend.1 = bf16[1024,128]{1,0:T(8,128)(2,1)} custom-call(s32[1]{0:T(128)} %bitcast.start, bf16[2048,256]{1,0:T(8,128)(2,1)S(1)} %bitcast.30), custom_call_target="tpu_custom_call" | custom-call | tf_op jit(solution)/shard_map/attend/pallas_call | solution.py:371
  39.9 4.2 %all-to-all-start.1 = ((bf16[16,64,128]{2,1,0:T(8,128)(2,1)}), bf16[16,64,128]{2,1,0:T(8,128)(2,1)S(1)}, u32[]{:S(2)}, u32[]{:S(2)}) async-start(bf16[16,64,128]{2,1,0:T(8,128)(2,1)} %bitcast.10), calls=%async_computation.1 | async-start | bytes 524288 | tf_op jit(solution)/shard_map/all_to_all | solution.py:441
  44.2 0.5 route.1
  44.7 7.0 %all-to-all-done.1 = bf16[16,64,128]{2,1,0:T(8,128)(2,1)S(1)} async-done(((bf16[16,64,128]{2,1,0:T(8,128)(2,1)}), bf16[16,64,128]{2,1,0:T(8,128)(2,1)S(1)}, u32[]{:S(2)}, u32[]{:S(2)}) %all-to-all-start.1) | async-done | bytes 262176 | tf_op jit(solution)/shard_map/all_to_all | solution.py:441
  51.7 0.0 copy-start
  51.8 2.2 %copy-done = bf16[1024,2048]{1,0:T(8,128)(2,1)S(1)} copy-done((bf16[1024,2048]{1,0:T(8,128)(2,1)S(1)}, bf16[1024,2048]{1,0:T(8,128)(2,1)}, u32[]{:S(2)}) %copy-start) | copy-done | bytes 4194328
  53.9 1.9 %mix.1 = (f32[128,2048]{1,0:T(8,128)S(1)}, bf16[1024,1024]{1,0:T(8,128)(2,1)S(1)}) custom-call(bf16[1024,128]{1,0:T(8,128)(2,1)S(1)} %bitcast.32, bf16[128,2048]{1,0:T(8,128)(2,1)S(1)} %bitcast.33, f32[1,1024]{1,0:T(1,128)S(1)} %bitcast.38, bf16[1024,2048]{1,0:T(8,128)(2,1)S(1)} %copy-done, f32[1,2048]{1,0:T(1,128)S(1)} %bitcast.37, ...), custom_call_target="tpu_custom_call" | custom-call | tf_op jit(solution)/shard_map/mix/pallas_call | solution.py:371
  55.9 38.3 %all_to_all.44 = bf16[128,8,1024]{2,1,0:T(8,128)(2,1)S(1)} all-to-all(bf16[128,8,1024]{2,1,0:T(8,128)(2,1)S(1)} %bitcast.31), channel_id=1, replica_groups=mesh['sp'=16,'dp'=8] {'sp','dp'}, dimensions={0} | all-to-all | bytes 4194304 | tf_op jit(solution)/shard_map/all_to_all | solution.py:449
  94.2 3.5 %expert.1 = bf16[1024,1024]{1,0:T(8,128)(2,1)S(1)} custom-call(bf16[1024,1024]{1,0:T(8,128)(2,1)S(1)} %bitcast.27, bf16[1,2048,512]{2,1,0:T(8,128)(2,1)S(1)} %copy-done.1, bf16[1,2048,512]{2,1,0:T(8,128)(2,1)S(1)} %copy-done.2, bf16[1,512,2048]{2,1,0:T(8,128)(2,1)S(1)} %copy-done.3), custom_call_target="tpu_custom_call" | custom-call | tf_op jit(solution)/shard_map/expert/pallas_call | solution.py:371
  97.7 34.4 %all_to_all.45 = bf16[128,8,1024]{2,1,0:T(8,128)(2,1)S(1)} all-to-all(bf16[128,8,1024]{2,1,0:T(8,128)(2,1)S(1)} %bitcast.28), channel_id=1, replica_groups=mesh['sp'=16,'dp'=8] {'sp','dp'}, dimensions={0} | all-to-all | bytes 4194304 | tf_op jit(solution)/shard_map/all_to_all | solution.py:457
  132.0 1.8 %combine.1 = bf16[128,2048]{1,0:T(8,128)(2,1)} custom-call(bf16[1024,1024]{1,0:T(8,128)(2,1)S(1)} %bitcast.29, bf16[256,512]{1,0:T(8,128)(2,1)S(1)} %get-tuple-element.12.gather, f32[128,2048]{1,0:T(8,128)S(1)} %get-tuple-element.13.stream, f32[128,2]{1,0:T(8,128)S(1)} %get-tuple-element.14.route_weight), custom_call_target="tpu_custom_call" | custom-call | tf_op jit(solution)/shard_map/combine/pallas_call | solution.py:371
  (27 shorter events, 0.1 us)
Async XLA Ops:
  0.3 1.0 copy-start.5
  1.4 1.0 copy-start.6
  2.4 1.0 copy-start.7
  3.4 0.8 copy-start.8
  4.3 0.7 copy-start.9
  5.0 0.7 copy-start.12
  5.6 0.7 copy-start.15
  6.3 0.7 copy-start.16
  9.6 34.5 %copy-start.13 = (s32[1,128,2]{1,2,0:T(2,128)S(1)}, s32[1,128,2]{1,2,0:T(2,128)}, u32[]{:S(2)}) copy-start(s32[1,128,2]{1,2,0:T(2,128)} %param.30) | copy-start | bytes 3076
  9.6 34.5 %copy-start.14 = (f32[1,128,2]{1,2,0:T(2,128)S(1)}, f32[1,128,2]{1,2,0:T(2,128)}, u32[]{:S(2)}) copy-start(f32[1,128,2]{1,2,0:T(2,128)} %param.32) | copy-start | bytes 3076
  9.6 34.6 %copy-start.17 = (f32[1,128]{1,0:T(1,128)S(1)}, f32[1,128]{1,0:T(1,128)}, u32[]{:S(2)}) copy-start(f32[1,128]{1,0:T(1,128)} %group_prob.1) | copy-start | bytes 1540
  9.6 42.1 %copy-start.4 = (bf16[1,128,2048]{2,1,0:T(8,128)(2,1)S(1)}, bf16[1,128,2048]{2,1,0:T(8,128)(2,1)}, u32[]{:S(2)}) copy-start(bf16[1,128,2048]{2,1,0:T(8,128)(2,1)} %param.18) | copy-start | bytes 1572868
  9.6 42.1 %copy-start.10 = (f32[2048]{0:T(1024)S(1)}, f32[2048]{0:T(1024)}, u32[]{:S(2)}) copy-start(f32[2048]{0:T(1024)} %param.29) | copy-start | bytes 24580
  9.6 42.1 %copy-start.11 = (f32[1024]{0:T(1024)S(1)}, f32[1024]{0:T(1024)}, u32[]{:S(2)}) copy-start(f32[1024]{0:T(1024)} %param.27) | copy-start | bytes 12292
  9.6 24.8 %all-to-all-start = ((bf16[16,128,256]{2,1,0:T(8,128)(2,1)}), bf16[16,128,256]{2,1,0:T(8,128)(2,1)S(1)}, u32[]{:S(2)}, u32[]{:S(2)}) async-start(bf16[16,128,256]{2,1,0:T(8,128)(2,1)} %bitcast.8), calls=%async_computation | async-start | bytes 2097152 | tf_op jit(solution)/shard_map/all_to_all | solution.py:426
  39.9 11.8 %all-to-all-start.1 = ((bf16[16,64,128]{2,1,0:T(8,128)(2,1)}), bf16[16,64,128]{2,1,0:T(8,128)(2,1)S(1)}, u32[]{:S(2)}, u32[]{:S(2)}) async-start(bf16[16,64,128]{2,1,0:T(8,128)(2,1)} %bitcast.10), calls=%async_computation.1 | async-start | bytes 524288 | tf_op jit(solution)/shard_map/all_to_all | solution.py:441
  51.7 2.2 %copy-start = (bf16[1024,2048]{1,0:T(8,128)(2,1)S(1)}, bf16[1024,2048]{1,0:T(8,128)(2,1)}, u32[]{:S(2)}) copy-start(bf16[1024,2048]{1,0:T(8,128)(2,1)} %out_weight.1) | copy-start | bytes 12582916
  53.9 40.2 %copy-start.3 = (bf16[1,512,2048]{2,1,0:T(8,128)(2,1)S(1)}, bf16[1,512,2048]{2,1,0:T(8,128)(2,1)}, u32[]{:S(2)}) copy-start(bf16[1,512,2048]{2,1,0:T(8,128)(2,1)} %down_weight.1) | copy-start | bytes 6291460
  55.8 38.3 %copy-start.1 = (bf16[1,2048,512]{2,1,0:T(8,128)(2,1)S(1)}, bf16[1,2048,512]{2,1,0:T(8,128)(2,1)}, u32[]{:S(2)}) copy-start(bf16[1,2048,512]{2,1,0:T(8,128)(2,1)} %gate_weight.1) | copy-start | bytes 6291460
  55.8 38.3 %copy-start.2 = (bf16[1,2048,512]{2,1,0:T(8,128)(2,1)S(1)}, bf16[1,2048,512]{2,1,0:T(8,128)(2,1)}, u32[]{:S(2)}) copy-start(bf16[1,2048,512]{2,1,0:T(8,128)(2,1)} %up_weight.1) | copy-start | bytes 6291460

commit v3 on v2

--- a/solution.py
+++ b/solution.py
@@ -57,9 +57,40 @@
     key_weight,
     value_weight,
     out,
+    query_here,
+    latent_here,
+    rope_here,
+    latent_gain_here,
+    query_gain_here,
+    key_gain_here,
+    key_weight_here,
+    value_weight_here,
+    arrivals,
     small,
     turn,
 ):
+    moves = [
+        pltpu.make_async_copy(source, target, arrivals.at[k])
+        for k, (source, target) in enumerate(
+            (
+                (query_gain, query_gain_here),
+                (key_gain, key_gain_here),
+                (rope, rope_here),
+                (latent_gain, latent_gain_here),
+                (latent, latent_here),
+                (key_weight, key_weight_here),
+                (value_weight, value_weight_here),
+                (query, query_here),
+            )
+        )
+    ]
+    for move in moves:
+        move.start()
+    for move in moves:
+        move.wait()
+    query, latent, rope, latent_gain = query_here, latent_here, rope_here, latent_gain_here
+    query_gain, key_gain = query_gain_here, key_gain_here
+    key_weight, value_weight = key_weight_here, value_weight_here
     rows = query.shape[0]
     heads = query.shape[1] // 96
     lane = lane_iota(rows)
@@ -190,11 +221,49 @@
                 )
 
 
-def attend_kernel(start, packed, out):
+def attend_kernel(
+    packed,
+    choice,
+    group_prob,
+    shares,
+    out_weight,
+    gate_weight,
+    up_weight,
+    down_weight,
+    out,
+    spread,
+    gather,
+    weight,
+    out_weight_here,
+    gate_weight_here,
+    up_weight_here,
+    down_weight_here,
+    arrivals,
+):
+    moves = [
+        pltpu.make_async_copy(source, target, arrivals.at[k])
+        for k, (source, target) in enumerate(
+            (
+                (out_weight, out_weight_here),
+                (gate_weight, gate_weight_here),
+                (up_weight, up_weight_here),
+                (down_weight, down_weight_here),
+            )
+        )
+    ]
+    for move in moves:
+        move.start()
+    route(choice, group_prob, shares, spread, gather, weight)
+    attend(packed, out)
+    for move in moves:
+        move.wait()
+
+
+def attend(packed, out):
     length = packed.shape[0]
     rows = 256
-    scale = 96 ** (-0.5)
-    begin = start[0]
+    scale = 96 ** (-0.5) * 1.4426950408889634
+    begin = (lax.axis_index("sp") * 96) % 128
     keep = (((lane_iota(16) - begin + 128) % 128) < 96).astype(jnp.float32).astype(jnp.bfloat16)[0:1]
     query_seg = lax.broadcasted_iota(jnp.int32, (rows, rows), 0) // SPAN
     key_seg = lax.broadcasted_iota(jnp.int32, (rows, rows), 1) // SPAN
@@ -223,7 +292,7 @@
         else:
             scores = own
         top = jnp.max(fold(scores, jnp.maximum), axis=-1, keepdims=True)
-        raised = jnp.exp((scores - top) * scale)
+        raised = jnp.exp2(scores * scale - top * scale)
         row_sum = jnp.sum(fold(raised, jnp.add), axis=-1, keepdims=True)
         summed = jnp.dot(
             raised.astype(jnp.bfloat16), packed[0:last, :], preferred_element_type=jnp.float32
@@ -249,7 +318,7 @@
             out[at : at + 64, :] = joined.astype(jnp.bfloat16)
 
 
-def route_kernel(choice, group_prob, shares, spread, gather, weight):
+def route(choice, group_prob, shares, spread, gather, weight):
     tokens = choice.shape[1]
     expert = lax.broadcasted_iota(jnp.int32, (LANES, tokens), 0)
     first = choice[0:1, :]
@@ -359,25 +428,31 @@
     out[...] = (stream[...] + routed).astype(jnp.bfloat16)
 
 
-def call(body, out_shapes, mib, scratch=(), name=None, scalars=0):
-    spec = [pl.BlockSpec(memory_space=pltpu.SMEM)] * scalars
-    extra = {}
-
-    def run(*operands):
-        if scalars:
-            extra["in_specs"] = spec + [
-                pl.BlockSpec(memory_space=pltpu.VMEM) for _ in operands[scalars:]
-            ]
-        return pl.pallas_call(
-            body,
-            out_shape=out_shapes,
-            scratch_shapes=list(scratch),
-            compiler_params=pltpu.CompilerParams(vmem_limit_bytes=mib * 2**20),
-            name=name,
-            **extra,
-        )(*operands)
-
-    return run
+VMEM = pl.BlockSpec(memory_space=pltpu.VMEM)
+HBM = pl.BlockSpec(memory_space=pltpu.HBM)
+
+
+def call(body, in_specs, out_shapes, mib, scratch=(), name=None):
+    many = isinstance(out_shapes, tuple)
+    run = pl.pallas_call(
+        body,
+        in_specs=in_specs,
+        out_shape=out_shapes,
+        out_specs=tuple(VMEM for _ in out_shapes) if many else VMEM,
+        scratch_shapes=list(scratch),
+        compiler_params=pltpu.CompilerParams(vmem_limit_bytes=mib * 2**20),
+        name=name,
+    )
+
+    def placed(*operands):
+        return run(
+            *(
+                pltpu.with_memory_space_constraint(x, pltpu.HBM) if spec is HBM else x
+                for spec, x in zip(in_specs, operands)
+            )
+        )
+
+    return placed
 
 
 def per_device(
@@ -405,11 +480,25 @@
     sequence = tokens * lax.axis_size("sp")
     shape = jax.ShapeDtypeStruct
     phases = angles(lax.axis_index("sp") * tokens, tokens, rope_key.shape[2])
+    half = jnp.bfloat16
     packed = call(
         project_kernel,
-        shape((16 * tokens, 256), jnp.bfloat16),
-        12,
-        scratch=(pltpu.VMEM((16, 128), jnp.float32), pltpu.VMEM((tokens, 384), jnp.float32)),
+        [HBM] * 6 + [VMEM] * 2 + [HBM] * 2,
+        shape((16 * tokens, 256), half),
+        14,
+        scratch=(
+            pltpu.VMEM(query.shape[1:], half),
+            pltpu.VMEM(latent.shape[1:], half),
+            pltpu.VMEM(rope_key.shape[:0:-1], half),
+            pltpu.VMEM((1,) + latent_gain.shape, jnp.float32),
+            pltpu.VMEM((1,) + query_gain.shape, jnp.float32),
+            pltpu.VMEM((1,) + key_gain.shape, jnp.float32),
+            pltpu.VMEM(key_weight.shape, half),
+            pltpu.VMEM(value_weight.shape, half),
+            pltpu.SemaphoreType.DMA((8,)),
+            pltpu.VMEM((16, 128), jnp.float32),
+            pltpu.VMEM((tokens, 384), jnp.float32),
+        ),
         name="project",
     )(
         query[0],
@@ -424,24 +513,37 @@
         value_weight,
     )
     by_head = lax.all_to_all(packed, "sp", split_axis=0, concat_axis=0, tiled=True)
-    spread, gather, route_weight = call(
-        route_kernel,
+    head_out, spread, gather, route_weight, out_weight, gate_weight, up_weight, down_weight = call(
+        attend_kernel,
+        [VMEM] * 4 + [HBM] * 4,
         (
-            shape((1024, 256), jnp.bfloat16),
-            shape((256, 512), jnp.bfloat16),
+            shape((sequence // 2, 128), half),
+            shape((1024, 256), half),
+            shape((256, 512), half),
             shape((tokens, 2), jnp.float32),
+            shape(out_weight.shape, half),
+            shape(gate_weight.shape, half),
+            shape(up_weight.shape, half),
+            shape(down_weight.shape, half),
         ),
-        8,
-        name="route",
-    )(expert_choice[0].T, group_prob, expert_prob[0].T)
-    start = (lax.axis_index("sp") * 96) % 128
-    head_out = call(
-        attend_kernel, shape((sequence // 2, 128), jnp.bfloat16), 20, name="attend", scalars=1
-    )(start[None].astype(jnp.int32), by_head)
+        30,
+        scratch=(pltpu.SemaphoreType.DMA((4,)),),
+        name="attend",
+    )(
+        by_head,
+        expert_choice[0].T,
+        group_prob,
+        expert_prob[0].T,
+        out_weight,
+        gate_weight,
+        up_weight,
+        down_weight,
+    )
     by_token = lax.all_to_all(head_out, "sp", split_axis=0, concat_axis=0, tiled=True)
     stream, outgoing = call(
         mix_kernel,
-        (shape((tokens, width), jnp.float32), shape((1024, 1024), jnp.bfloat16)),
+        [VMEM] * 6,
+        (shape((tokens, width), jnp.float32), shape((1024, 1024), half)),
         16,
         scratch=(pltpu.VMEM((tokens, 1024), jnp.float32),),
         name="mix",
@@ -449,17 +551,19 @@
     arrived = lax.all_to_all(outgoing, ("sp", "dp"), split_axis=0, concat_axis=0, tiled=True)
     answers = call(
         expert_kernel,
-        shape((1024, 1024), jnp.bfloat16),
+        [VMEM] * 4,
+        shape((1024, 1024), half),
         20,
-        scratch=(pltpu.VMEM((512, width), jnp.bfloat16),),
+        scratch=(pltpu.VMEM((512, width), half),),
         name="expert",
     )(arrived, gate_weight, up_weight, down_weight)
     returned = lax.all_to_all(answers, ("sp", "dp"), split_axis=0, concat_axis=0, tiled=True)
     return call(
         combine_kernel,
-        shape((tokens, width), jnp.bfloat16),
+        [VMEM] * 4,
+        shape((tokens, width), half),
         14,
-        scratch=(pltpu.VMEM((512, width), jnp.bfloat16),),
+        scratch=(pltpu.VMEM((512, width), half),),
         name="combine",
     )(returned, gather, stream, route_weight)[None]
 

time: 134 us -> 127 us (0.948)
  blocking collectives: 72.6 us -> 108 us
  waiting for transfers between devices: 23 us -> 0 us
  starting transfers between devices: 12.9 us -> 0 us
  local copies, waits for them, and re-layouts: 8.82 us -> 0.04 us
  Pallas kernels: 15.9 us -> 18.4 us
    all_to_all x0 -> x2, blocking collectives: none -> 35.4 us  [the longest x1 24.4 us: per_device(): lax.all_to_all(packed, 'sp', split_axis=0, concat_axis=0, tiled=True)]
    all_to_all x2 -> x0, waiting for transfers between devices: 23 us -> none  [the longest x1 16 us: per_device(): lax.all_to_all(packed, 'sp', split_axis=0, concat_axis=0, tiled=True)]
    all_to_all x2 -> x0, starting transfers between devices: 12.9 us -> none  [the longest x1 8.73 us: per_device(): lax.all_to_all(packed, 'sp', split_axis=0, concat_axis=0, tiled=True)]
    unnamed x36 -> x12, local copies, waits for them, and re-layouts: 8.82 us -> 0.04 us
    pallas_call x6 -> x5, Pallas kernels: 15.9 us -> 18.4 us  [placed(): run(*(pltpu.with_memory_space_constraint(x, pltpu.HBM) if spec is HBM els...]
  transfers between devices with their start and end apart: 2 -> 0, of which waited for: 2 -> 0; matrix products, arithmetic and copies ran while one was open for 0% -> 0% of each run, Pallas kernels for 0% -> 0%
where the time goes in v3:
time: 127 us
  blocking collectives  108 us (85%)
  Pallas kernels  18.4 us (14%)
    all_to_all x1, blocking collectives, per_device(): lax.all_to_all(outgoing, ('sp', 'dp'), split_axis=0, concat_axis=0, tiled...  38 us
    all_to_all x1, blocking collectives, per_device(): lax.all_to_all(answers, ('sp', 'dp'), split_axis=0, concat_axis=0, tiled=...  34.4 us
    all_to_all x1, blocking collectives, per_device(): lax.all_to_all(packed, 'sp', split_axis=0, concat_axis=0, tiled=True)  24.4 us
    pallas_call x5, Pallas kernels, placed(): run(*(pltpu.with_memory_space_constraint(x, pltpu.HBM) if spec is HBM els...  18.4 us
    all_to_all x1, blocking collectives, per_device(): lax.all_to_all(head_out, 'sp', split_axis=0, concat_axis=0, tiled=True)  11 us

profile of v3, /device:TPU:1, one launch (start us, length us, event | category | flops | bytes accessed | tf_op | source)
XLA Modules:
  0.0 126.7 jit_solution(5996823144250263756)
XLA Ops:
  0.0 0.3 multiply_sine_fusion
  0.3 0.0 copy-start.3
  0.4 0.0 copy-start.4
  0.4 0.0 copy-start.5
  0.4 3.1 %project.1 = bf16[2048,256]{1,0:T(8,128)(2,1)S(1)} custom-call(bf16[128,1536]{1,0:T(8,128)(2,1)} %bitcast.39, bf16[128,256]{1,0:T(8,128)(2,1)} %bitcast.40, bf16[32,128]{1,0:T(8,128)(2,1)} %bitcast.41, f32[1,256]{1,0:T(1,128)} %bitcast.42, f32[1,96]{1,0:T(1,128)} %bitcast.43, f32[1,96]{1,0:T(1,128)} %bitcast.44, f32[128,16]{1,0:T(8,128)S(1)} %get-tuple-element.26.cos_table, ...), custom_call_target="tpu_custom_call" | custom-call | tf_op jit(solution)/shard_map/project/pallas_call | solution.py:448
  3.5 24.4 %all_to_all.44 = bf16[16,128,256]{2,1,0:T(8,128)(2,1)S(1)} all-to-all(bf16[16,128,256]{2,1,0:T(8,128)(2,1)S(1)} %bitcast.30), channel_id=1, replica_groups=mesh['sp'=16,'dp'=8] {'sp'}, dimensions={0} | all-to-all | bytes 2097152 | tf_op jit(solution)/shard_map/all_to_all | solution.py:515
  28.0 0.0 copy-done.3
  28.0 0.0 copy-done.4
  28.0 0.0 copy-done.5
  28.0 0.0 copy-start
  28.0 0.0 copy-start.1
  28.0 0.0 copy-start.2
  28.0 7.9 %attend.1 = (bf16[1024,128]{1,0:T(8,128)(2,1)S(1)}, bf16[1024,256]{1,0:T(8,128)(2,1)S(1)}, bf16[256,512]{1,0:T(8,128)(2,1)S(1)}, f32[128,2]{1,0:T(8,128)S(1)}, b...) custom-call(bf16[2048,256]{1,0:T(8,128)(2,1)S(1)} %bitcast.29, ...), custom_call_target="tpu_custom_call" | custom-call | tf_op jit(solution)/shard_map/attend/pallas_call | solution.py:448
  35.9 11.0 %all_to_all.45 = bf16[16,64,128]{2,1,0:T(8,128)(2,1)S(1)} all-to-all(bf16[16,64,128]{2,1,0:T(8,128)(2,1)S(1)} %bitcast.34), channel_id=1, replica_groups=mesh['sp'=16,'dp'=8] {'sp'}, dimensions={0} | all-to-all | bytes 524288 | tf_op jit(solution)/shard_map/all_to_all | solution.py:542
  46.9 0.0 copy-done
  46.9 0.0 copy-done.1
  46.9 0.0 copy-done.2
  46.9 1.9 %mix.1 = (f32[128,2048]{1,0:T(8,128)S(1)}, bf16[1024,1024]{1,0:T(8,128)(2,1)S(1)}) custom-call(bf16[1024,128]{1,0:T(8,128)(2,1)S(1)} %bitcast.32, bf16[128,2048]{1,0:T(8,128)(2,1)S(1)} %bitcast.33, f32[1,1024]{1,0:T(1,128)S(1)} %bitcast.36, bf16[1024,2048]{1,0:T(8,128)(2,1)S(1)} %get-tuple-element.16.out_weight, f32[1,2048]{1,0:T(1,128)S(1)} %bitcast.35, ...), custom_call_target="tpu_custom_call" | custom-call | tf_op jit(solution)/shard_map/mix/pallas_call | solution.py:448
  48.8 38.0 %all_to_all.46 = bf16[128,8,1024]{2,1,0:T(8,128)(2,1)S(1)} all-to-all(bf16[128,8,1024]{2,1,0:T(8,128)(2,1)S(1)} %bitcast.31), channel_id=1, replica_groups=mesh['sp'=16,'dp'=8] {'sp','dp'}, dimensions={0} | all-to-all | bytes 4194304 | tf_op jit(solution)/shard_map/all_to_all | solution.py:551
  86.8 3.6 %expert.1 = bf16[1024,1024]{1,0:T(8,128)(2,1)S(1)} custom-call(bf16[1024,1024]{1,0:T(8,128)(2,1)S(1)} %bitcast.26, bf16[1,2048,512]{2,1,0:T(8,128)(2,1)S(1)} %get-tuple-element.19.gate_weight, bf16[1,2048,512]{2,1,0:T(8,128)(2,1)S(1)} %get-tuple-element.20.up_weight, bf16[1,512,2048]{2,1,0:T(8,128)(2,1)S(1)} %get-tuple-element.21.down_weight), custom_call_target="tpu_custom_call" | custom-call | tf_op jit(solution)/shard_map/expert/pallas_call | solution.py:448
  90.5 34.4 %all_to_all.47 = bf16[128,8,1024]{2,1,0:T(8,128)(2,1)S(1)} all-to-all(bf16[128,8,1024]{2,1,0:T(8,128)(2,1)S(1)} %bitcast.27), channel_id=1, replica_groups=mesh['sp'=16,'dp'=8] {'sp','dp'}, dimensions={0} | all-to-all | bytes 4194304 | tf_op jit(solution)/shard_map/all_to_all | solution.py:560
  124.8 1.8 %combine.1 = bf16[128,2048]{1,0:T(8,128)(2,1)} custom-call(bf16[1024,1024]{1,0:T(8,128)(2,1)S(1)} %bitcast.28, bf16[256,512]{1,0:T(8,128)(2,1)S(1)} %get-tuple-element.22.gather, f32[128,2048]{1,0:T(8,128)S(1)} %get-tuple-element.23.stream, f32[128,2]{1,0:T(8,128)S(1)} %get-tuple-element.24.route_weight), custom_call_target="tpu_custom_call" | custom-call | tf_op jit(solution)/shard_map/combine/pallas_call | solution.py:448
  (2 shorter events, 0.0 us)
Async XLA Ops:
  0.3 27.6 %copy-start.3 = (s32[1,128,2]{1,2,0:T(2,128)S(1)}, s32[1,128,2]{1,2,0:T(2,128)}, u32[]{:S(2)}) copy-start(s32[1,128,2]{1,2,0:T(2,128)} %param.30) | copy-start | bytes 3076
  0.4 27.6 %copy-start.4 = (f32[1,128,2]{1,2,0:T(2,128)S(1)}, f32[1,128,2]{1,2,0:T(2,128)}, u32[]{:S(2)}) copy-start(f32[1,128,2]{1,2,0:T(2,128)} %param.32) | copy-start | bytes 3076
  0.4 27.6 %copy-start.5 = (f32[1,128]{1,0:T(1,128)S(1)}, f32[1,128]{1,0:T(1,128)}, u32[]{:S(2)}) copy-start(f32[1,128]{1,0:T(1,128)} %group_prob.1) | copy-start | bytes 1540
  28.0 18.9 %copy-start = (bf16[1,128,2048]{2,1,0:T(8,128)(2,1)S(1)}, bf16[1,128,2048]{2,1,0:T(8,128)(2,1)}, u32[]{:S(2)}) copy-start(bf16[1,128,2048]{2,1,0:T(8,128)(2,1)} %param.18) | copy-start | bytes 1572868
  28.0 18.9 %copy-start.1 = (f32[2048]{0:T(1024)S(1)}, f32[2048]{0:T(1024)}, u32[]{:S(2)}) copy-start(f32[2048]{0:T(1024)} %param.29) | copy-start | bytes 24580
  28.0 18.9 %copy-start.2 = (f32[1024]{0:T(1024)S(1)}, f32[1024]{0:T(1024)}, u32[]{:S(2)}) copy-start(f32[1024]{0:T(1024)} %param.27) | copy-start | bytes 12292

commit v4 on v3

--- a/solution.py
+++ b/solution.py
@@ -86,7 +86,7 @@
     ]
     for move in moves:
         move.start()
-    for move in moves:
+    for move in moves[:3]:
         move.wait()
     query, latent, rope, latent_gain = query_here, latent_here, rope_here, latent_gain_here
     query_gain, key_gain = query_gain_here, key_gain_here
@@ -94,17 +94,6 @@
     rows = query.shape[0]
     heads = query.shape[1] // 96
     lane = lane_iota(rows)
-    raw_latent = latent[...].astype(jnp.float32)
-    normed_latent = (
-        raw_latent * inverse_rms(raw_latent, raw_latent.shape[1]) * latent_gain[...]
-    ).astype(jnp.bfloat16)
-    key_part = (
-        jnp.dot(normed_latent, key_weight[...], preferred_element_type=jnp.float32)
-        .astype(jnp.bfloat16)
-        .astype(jnp.float32)
-    )
-    values = jnp.dot(normed_latent, value_weight[...], preferred_element_type=jnp.float32)
-
     small[...] = jnp.zeros(small.shape, jnp.float32)
     small[0:1, 0:96] = query_gain[...]
     small[8:9, 0:96] = key_gain[...]
@@ -152,6 +141,20 @@
     rope_turned = turn_lanes(rope_part * key_gain_row, *tables)
     rope_at = [rope_turned] + [pltpu.roll(rope_turned, shift, 1) for shift in (96, 64, 32)]
     low_gain = jnp.where(lane_iota(8) < 64, small[8:16, :], pltpu.roll(small[8:16, :], 64, 1))[0:1]
+
+    for move in moves[3:7]:
+        move.wait()
+    raw_latent = latent[...].astype(jnp.float32)
+    normed_latent = (
+        raw_latent * inverse_rms(raw_latent, raw_latent.shape[1]) * latent_gain[...]
+    ).astype(jnp.bfloat16)
+    key_part = (
+        jnp.dot(normed_latent, key_weight[...], preferred_element_type=jnp.float32)
+        .astype(jnp.bfloat16)
+        .astype(jnp.float32)
+    )
+    values = jnp.dot(normed_latent, value_weight[...], preferred_element_type=jnp.float32)
+    moves[7].wait()
 
     for four in range(heads // 4):
         raw = [
@@ -227,36 +230,18 @@
     group_prob,
     shares,
     out_weight,
-    gate_weight,
-    up_weight,
-    down_weight,
     out,
     spread,
     gather,
     weight,
     out_weight_here,
-    gate_weight_here,
-    up_weight_here,
-    down_weight_here,
-    arrivals,
+    arrival,
 ):
-    moves = [
-        pltpu.make_async_copy(source, target, arrivals.at[k])
-        for k, (source, target) in enumerate(
-            (
-                (out_weight, out_weight_here),
-                (gate_weight, gate_weight_here),
-                (up_weight, up_weight_here),
-                (down_weight, down_weight_here),
-            )
-        )
-    ]
-    for move in moves:
-        move.start()
+    move = pltpu.make_async_copy(out_weight, out_weight_here, arrival)
+    move.start()
     route(choice, group_prob, shares, spread, gather, weight)
     attend(packed, out)
-    for move in moves:
-        move.wait()
+    move.wait()
 
 
 def attend(packed, out):
@@ -277,20 +262,24 @@
             parts = [combine(*parts[at : at + 2]) if at + 1 < len(parts) else parts[at] for at in range(0, len(parts), 2)]
         return parts[0]
 
-    for block in range(length // rows):
+    def scores_of(block):
         first, last = block * rows, (block + 1) * rows
-        head_query = packed[first:last, 0:128] * keep
-        scores = lax.dot_general(
-            head_query,
+        return lax.dot_general(
+            packed[first:last, 0:128] * keep,
             packed[0:last, 128:256],
             (((1,), (1,)), ((), ())),
             preferred_element_type=jnp.float32,
         )
+
+    blocks = length // rows
+    coming = scores_of(blocks - 1)
+    for block in range(blocks - 1, -1, -1):
+        first, last = block * rows, (block + 1) * rows
+        scores = coming
+        if block:
+            coming = scores_of(block - 1)
         own = jnp.where(allowed, scores[:, first:last], -1e30)
-        if block:
-            scores = jnp.concatenate([scores[:, :first], own], axis=1)
-        else:
-            scores = own
+        scores = jnp.concatenate([scores[:, :first], own], axis=1) if block else own
         top = jnp.max(fold(scores, jnp.maximum), axis=-1, keepdims=True)
         raised = jnp.exp2(scores * scale - top * scale)
         row_sum = jnp.sum(fold(raised, jnp.add), axis=-1, keepdims=True)
@@ -513,32 +502,20 @@
         value_weight,
     )
     by_head = lax.all_to_all(packed, "sp", split_axis=0, concat_axis=0, tiled=True)
-    head_out, spread, gather, route_weight, out_weight, gate_weight, up_weight, down_weight = call(
+    head_out, spread, gather, route_weight, out_weight = call(
         attend_kernel,
-        [VMEM] * 4 + [HBM] * 4,
+        [VMEM] * 4 + [HBM],
         (
             shape((sequence // 2, 128), half),
             shape((1024, 256), half),
             shape((256, 512), half),
             shape((tokens, 2), jnp.float32),
             shape(out_weight.shape, half),
-            shape(gate_weight.shape, half),
-            shape(up_weight.shape, half),
-            shape(down_weight.shape, half),
         ),
-        30,
-        scratch=(pltpu.SemaphoreType.DMA((4,)),),
+        24,
+        scratch=(pltpu.SemaphoreType.DMA,),
         name="attend",
-    )(
-        by_head,
-        expert_choice[0].T,
-        group_prob,
-        expert_prob[0].T,
-        out_weight,
-        gate_weight,
-        up_weight,
-        down_weight,
-    )
+    )(by_head, expert_choice[0].T, group_prob, expert_prob[0].T, out_weight)
     by_token = lax.all_to_all(head_out, "sp", split_axis=0, concat_axis=0, tiled=True)
     stream, outgoing = call(
         mix_kernel,

time: 127 us -> 123 us (0.969)
  Pallas kernels: 18.4 us -> 14.6 us
    pallas_call x5, Pallas kernels: 18.4 us -> 14.6 us  [placed(): run(*(pltpu.with_memory_space_constraint(x, pltpu.HBM) if spec is HBM els...]
where the time goes in v4:
time: 123 us
  blocking collectives  108 us (88%)
  Pallas kernels  14.6 us (12%)
    all_to_all x1, blocking collectives, per_device(): lax.all_to_all(outgoing, ('sp', 'dp'), split_axis=0, concat_axis=0, tiled...  38 us
    all_to_all x1, blocking collectives, per_device(): lax.all_to_all(answers, ('sp', 'dp'), split_axis=0, concat_axis=0, tiled=...  34.3 us
    all_to_all x1, blocking collectives, per_device(): lax.all_to_all(packed, 'sp', split_axis=0, concat_axis=0, tiled=True)  24.4 us
    pallas_call x5, Pallas kernels, placed(): run(*(pltpu.with_memory_space_constraint(x, pltpu.HBM) if spec is HBM els...  14.6 us
    all_to_all x1, blocking collectives, per_device(): lax.all_to_all(head_out, 'sp', split_axis=0, concat_axis=0, tiled=True)  11 us

profile of v4, /device:TPU:1, one launch (start us, length us, event | category | flops | bytes accessed | tf_op | source)
XLA Modules:
  0.0 122.9 jit_solution(12983721160939798742)
XLA Ops:
  0.0 0.3 multiply_sine_fusion
  0.3 0.0 copy-start.6
  0.4 0.0 copy-start.7
  0.4 0.0 copy-start.8
  0.4 2.9 %project.1 = bf16[2048,256]{1,0:T(8,128)(2,1)S(1)} custom-call(bf16[128,1536]{1,0:T(8,128)(2,1)} %bitcast.39, bf16[128,256]{1,0:T(8,128)(2,1)} %bitcast.40, bf16[32,128]{1,0:T(8,128)(2,1)} %bitcast.41, f32[1,256]{1,0:T(1,128)} %bitcast.42, f32[1,96]{1,0:T(1,128)} %bitcast.43, f32[1,96]{1,0:T(1,128)} %bitcast.44, f32[128,16]{1,0:T(8,128)S(1)} %get-tuple-element.20.cos_table, ...), custom_call_target="tpu_custom_call" | custom-call | tf_op jit(solution)/shard_map/project/pallas_call | solution.py:437
  3.3 24.4 %all_to_all.44 = bf16[16,128,256]{2,1,0:T(8,128)(2,1)S(1)} all-to-all(bf16[16,128,256]{2,1,0:T(8,128)(2,1)S(1)} %bitcast.30), channel_id=1, replica_groups=mesh['sp'=16,'dp'=8] {'sp'}, dimensions={0} | all-to-all | bytes 2097152 | tf_op jit(solution)/shard_map/all_to_all | solution.py:504
  27.7 0.0 copy-done.6
  27.7 0.0 copy-done.7
  27.7 0.0 copy-done.8
  27.8 0.0 copy-start.3
  27.8 0.0 copy-start.4
  27.8 0.0 copy-start.5
  27.8 4.4 %attend.1 = (bf16[1024,128]{1,0:T(8,128)(2,1)S(1)}, bf16[1024,256]{1,0:T(8,128)(2,1)S(1)}, bf16[256,512]{1,0:T(8,128)(2,1)S(1)}, f32[128,2]{1,0:T(8,128)S(1)}, bf16[1024,2048]{1,0:T(8,128)(2,1)S(1)}) custom-call(bf16[2048,256]{1,0:T(8,128)(2,1)S(1)} %bitcast.29, s32[2,128]{1,0:T(2,128)S(1)} %bitcast.37, f32[1,128]{1,0:T(1,128)S(1)} %copy-done.8, ...), custom_call_target="tpu_custom_call" | custom-call | tf_op jit(solution)/shard_map/attend/pallas_call | solution.py:437
  32.2 11.0 %all_to_all.45 = bf16[16,64,128]{2,1,0:T(8,128)(2,1)S(1)} all-to-all(bf16[16,64,128]{2,1,0:T(8,128)(2,1)S(1)} %bitcast.34), channel_id=1, replica_groups=mesh['sp'=16,'dp'=8] {'sp'}, dimensions={0} | all-to-all | bytes 524288 | tf_op jit(solution)/shard_map/all_to_all | solution.py:519
  43.2 0.0 copy-done.3
  43.2 0.0 copy-start.2
  43.2 1.9 %mix.1 = (f32[128,2048]{1,0:T(8,128)S(1)}, bf16[1024,1024]{1,0:T(8,128)(2,1)S(1)}) custom-call(bf16[1024,128]{1,0:T(8,128)(2,1)S(1)} %bitcast.32, bf16[128,2048]{1,0:T(8,128)(2,1)S(1)} %bitcast.33, f32[1,1024]{1,0:T(1,128)S(1)} %bitcast.36, bf16[1024,2048]{1,0:T(8,128)(2,1)S(1)} %get-tuple-element.13.out_weight, f32[1,2048]{1,0:T(1,128)S(1)} %bitcast.35, ...), custom_call_target="tpu_custom_call" | custom-call | tf_op jit(solution)/shard_map/mix/pallas_call | solution.py:437
  45.1 0.0 copy-start
  45.1 0.0 copy-start.1
  45.1 38.0 %all_to_all.46 = bf16[128,8,1024]{2,1,0:T(8,128)(2,1)S(1)} all-to-all(bf16[128,8,1024]{2,1,0:T(8,128)(2,1)S(1)} %bitcast.31), channel_id=1, replica_groups=mesh['sp'=16,'dp'=8] {'sp','dp'}, dimensions={0} | all-to-all | bytes 4194304 | tf_op jit(solution)/shard_map/all_to_all | solution.py:528
  83.1 0.0 copy-done.1
  83.1 3.5 %expert.1 = bf16[1024,1024]{1,0:T(8,128)(2,1)S(1)} custom-call(bf16[1024,1024]{1,0:T(8,128)(2,1)S(1)} %bitcast.26, bf16[1,2048,512]{2,1,0:T(8,128)(2,1)S(1)} %copy-done, bf16[1,2048,512]{2,1,0:T(8,128)(2,1)S(1)} %copy-done.1, bf16[1,512,2048]{2,1,0:T(8,128)(2,1)S(1)} %copy-done.2), custom_call_target="tpu_custom_call" | custom-call | tf_op jit(solution)/shard_map/expert/pallas_call | solution.py:437
  86.7 34.3 %all_to_all.47 = bf16[128,8,1024]{2,1,0:T(8,128)(2,1)S(1)} all-to-all(bf16[128,8,1024]{2,1,0:T(8,128)(2,1)S(1)} %bitcast.27), channel_id=1, replica_groups=mesh['sp'=16,'dp'=8] {'sp','dp'}, dimensions={0} | all-to-all | bytes 4194304 | tf_op jit(solution)/shard_map/all_to_all | solution.py:537
  121.0 1.8 %combine.1 = bf16[128,2048]{1,0:T(8,128)(2,1)} custom-call(bf16[1024,1024]{1,0:T(8,128)(2,1)S(1)} %bitcast.28, bf16[256,512]{1,0:T(8,128)(2,1)S(1)} %get-tuple-element.16.gather, f32[128,2048]{1,0:T(8,128)S(1)} %get-tuple-element.17.stream, f32[128,2]{1,0:T(8,128)S(1)} %get-tuple-element.18.route_weight), custom_call_target="tpu_custom_call" | custom-call | tf_op jit(solution)/shard_map/combine/pallas_call | solution.py:437
  (6 shorter events, 0.0 us)
Async XLA Ops:
  0.3 27.4 %copy-start.6 = (s32[1,128,2]{1,2,0:T(2,128)S(1)}, s32[1,128,2]{1,2,0:T(2,128)}, u32[]{:S(2)}) copy-start(s32[1,128,2]{1,2,0:T(2,128)} %param.30) | copy-start | bytes 3076
  0.4 27.4 %copy-start.7 = (f32[1,128,2]{1,2,0:T(2,128)S(1)}, f32[1,128,2]{1,2,0:T(2,128)}, u32[]{:S(2)}) copy-start(f32[1,128,2]{1,2,0:T(2,128)} %param.32) | copy-start | bytes 3076
  0.4 27.4 %copy-start.8 = (f32[1,128]{1,0:T(1,128)S(1)}, f32[1,128]{1,0:T(1,128)}, u32[]{:S(2)}) copy-start(f32[1,128]{1,0:T(1,128)} %group_prob.1) | copy-start | bytes 1540
  27.8 15.4 %copy-start.3 = (bf16[1,128,2048]{2,1,0:T(8,128)(2,1)S(1)}, bf16[1,128,2048]{2,1,0:T(8,128)(2,1)}, u32[]{:S(2)}) copy-start(bf16[1,128,2048]{2,1,0:T(8,128)(2,1)} %param.18) | copy-start | bytes 1572868
  27.8 15.4 %copy-start.4 = (f32[2048]{0:T(1024)S(1)}, f32[2048]{0:T(1024)}, u32[]{:S(2)}) copy-start(f32[2048]{0:T(1024)} %param.29) | copy-start | bytes 24580
  27.8 15.4 %copy-start.5 = (f32[1024]{0:T(1024)S(1)}, f32[1024]{0:T(1024)}, u32[]{:S(2)}) copy-start(f32[1024]{0:T(1024)} %param.27) | copy-start | bytes 12292
  43.2 40.0 %copy-start.2 = (bf16[1,512,2048]{2,1,0:T(8,128)(2,1)S(1)}, bf16[1,512,2048]{2,1,0:T(8,128)(2,1)}, u32[]{:S(2)}) copy-start(bf16[1,512,2048]{2,1,0:T(8,128)(2,1)} %down_weight.1) | copy-start | bytes 6291460
  45.1 38.1 %copy-start = (bf16[1,2048,512]{2,1,0:T(8,128)(2,1)S(1)}, bf16[1,2048,512]{2,1,0:T(8,128)(2,1)}, u32[]{:S(2)}) copy-start(bf16[1,2048,512]{2,1,0:T(8,128)(2,1)} %gate_weight.1) | copy-start | bytes 6291460
  45.1 38.0 %copy-start.1 = (bf16[1,2048,512]{2,1,0:T(8,128)(2,1)S(1)}, bf16[1,2048,512]{2,1,0:T(8,128)(2,1)}, u32[]{:S(2)}) copy-start(bf16[1,2048,512]{2,1,0:T(8,128)(2,1)} %up_weight.1) | copy-start | bytes 6291460

commit v5 on v1

v5 whole, which is shorter than its diff:
```python
import jax
import jax.numpy as jnp
from jax import lax
from jax.experimental import pallas as pl
from jax.experimental.pallas import tpu as pltpu
from jax.sharding import PartitionSpec as P

SPAN = 64
LANES = 128
SLOTS = 4

eps = 1e-06


def angles(offset, span_count, rope_width):
    position = (offset + jnp.arange(span_count, dtype=jnp.int32)).astype(jnp.float32)
    frequency = 10000.0 ** (-2.0 * jnp.arange(rope_width // 2, dtype=jnp.float32) / rope_width)
    return position[:, None] * frequency[None, :]


def lane_iota(rows, width=LANES):
    return lax.broadcasted_iota(jnp.int32, (rows, width), 1)


def inverse_rms(vector, width):
    return lax.rsqrt(jnp.sum(vector * vector, axis=-1, keepdims=True) * (1.0 / width) + eps)


def turn_lanes(vector, cos_part, minus_sin, plus_sin):
    return (
        vector * cos_part
        + pltpu.roll(vector, 112, 1) * minus_sin
        + pltpu.roll(vector, 16, 1) * plus_sin
    )


def split_high_low(vector):
    high = vector.astype(jnp.bfloat16)
    low = (vector - high.astype(jnp.float32)).astype(jnp.bfloat16)
    return jnp.concatenate([high, low], axis=1)


def same_group(group_of_row, group_of_lane):
    ones = (group_of_row == group_of_lane).astype(jnp.float32).astype(jnp.bfloat16)
    return jnp.concatenate([ones, ones], axis=0)


def route(choice, group_prob, shares, spread, gather, weight):
    tokens = choice.shape[1]
    expert = lax.broadcasted_iota(jnp.int32, (LANES, tokens), 0)
    first = choice[0:1, :]
    second = choice[1:2, :]
    hot_first = (expert == first).astype(jnp.float32)
    hot_second = (expert == second).astype(jnp.float32)
    earlier = (
        (lax.broadcasted_iota(jnp.int32, (tokens, tokens), 0) < lane_iota(tokens, tokens))
        .astype(jnp.float32)
        .astype(jnp.bfloat16)
    )
    count_first = jnp.dot(
        hot_first.astype(jnp.bfloat16), earlier, preferred_element_type=jnp.float32
    )
    count_second = jnp.dot(
        hot_second.astype(jnp.bfloat16), earlier, preferred_element_type=jnp.float32
    ) + jnp.sum(hot_first, axis=1, keepdims=True)
    rank_first = jnp.sum(count_first * hot_first, axis=0, keepdims=True).astype(jnp.int32)
    rank_second = jnp.sum(count_second * hot_second, axis=0, keepdims=True).astype(jnp.int32)
    row_first = first * 8 + rank_first
    row_second = second * 8 + rank_second
    slot_row = lax.broadcasted_iota(jnp.int32, (spread.shape[0], tokens), 0)
    for half in range(2):
        picked = (slot_row == row_first + 4 * half) | (slot_row == row_second + 4 * half)
        spread[:, half * 128 : half * 128 + 128] = picked.astype(jnp.float32).astype(jnp.bfloat16)
    wide = lane_iota(tokens, 512)

    def down(row):
        return jnp.broadcast_to(row.astype(jnp.float32), (tokens, tokens)).T[:, 0:1]

    for k, (chosen, rank) in enumerate(((first, rank_first), (second, rank_second))):
        target = down(chosen * SLOTS + rank).astype(jnp.int32)
        gather[k * tokens : (k + 1) * tokens, :] = (
            (target == wide).astype(jnp.float32).astype(jnp.bfloat16)
        )
    total = shares[0:1, :] + shares[1:2, :]
    weight[:, 0:1] = down(group_prob[...] * shares[0:1, :] / total)
    weight[:, 1:2] = down(group_prob[...] * shares[1:2, :] / total)


def start_moves(pairs, arrivals):
    moves = [
        pltpu.make_async_copy(source, target, arrivals.at[k])
        for k, (source, target) in enumerate(pairs)
    ]
    for move in moves:
        move.start()
    return moves


def pack_kernel(latent, rope, latent_gain, out, latent_here, rope_here, latent_gain_here, arrivals):
    moves = start_moves(
        ((latent_gain, latent_gain_here), (rope, rope_here), (latent, latent_here)), arrivals
    )
    for move in moves:
        move.wait()
    rows = latent_here.shape[0]
    raw = latent_here[...].astype(jnp.float32)
    normed = (raw * inverse_rms(raw, raw.shape[1]) * latent_gain_here[...]).astype(jnp.bfloat16)
    block = rows + 16
    first, second = rope_here[0:16, :], rope_here[16:32, :]
    for device in range(out.shape[0] // block):
        at = device * block
        out[at : at + rows, :] = normed
        out[at + rows : at + block, 0:128] = first
        out[at + rows : at + block, 128:256] = second


def query_kernel(
    query,
    query_gain,
    key_weight,
    cos_table,
    sin_table,
    choice,
    group_prob,
    shares,
    out,
    key_weight_turned,
    spread,
    gather,
    weight,
    query_here,
    query_gain_here,
    key_weight_here,
    arrivals,
    small,
    turn,
):
    moves = start_moves(
        (
            (query_gain, query_gain_here),
            (query, query_here),
            (key_weight, key_weight_here),
        ),
        arrivals,
    )
    route(choice, group_prob, shares, spread, gather, weight)
    query = query_here
    rows = query.shape[0]
    heads = query.shape[1] // 96
    lane = lane_iota(rows)
    early = lax.broadcasted_iota(jnp.int32, (rows, LANES), 0) < SPAN
    for move in moves:
        move.wait()
    key_weight_turned[...] = key_weight_here[...].astype(jnp.float32).T.astype(jnp.bfloat16)
    small[...] = jnp.zeros(small.shape, jnp.float32)
    small[0:1, 0:96] = query_gain_here[...]
    turn[:, 0:128] = jnp.ones((rows, 128), jnp.float32)
    turn[:, 128:384] = jnp.zeros((rows, 256), jnp.float32)
    turn[:, 64:80] = cos_table[...]
    turn[:, 80:96] = cos_table[...]
    turn[:, 192:208] = -sin_table[...]
    turn[:, 336:352] = sin_table[...]
    tables = [turn[:, 0:128], turn[:, 128:256], turn[:, 256:384]]
    gain_row = small[0:8, :]
    gain_tiles = [
        (gain_row + pltpu.roll(gain_row, 96, 1) * (lane_iota(8) >= 96).astype(jnp.float32))[0:1],
        jnp.where(lane_iota(8) < 64, pltpu.roll(gain_row, 96, 1), pltpu.roll(gain_row, 64, 1))[0:1],
        jnp.where(lane_iota(8) < 32, pltpu.roll(gain_row, 64, 1), pltpu.roll(gain_row, 32, 1))[0:1],
    ]
    turn_tiles = [
        tables,
        [pltpu.roll(t, 96, 1) for t in tables],
        [jnp.where(lane < 64, pltpu.roll(t, 64, 1), pltpu.roll(t, 32, 1)) for t in tables],
    ]
    wide_row = lax.broadcasted_iota(jnp.int32, (128, 256), 0)
    wide_lane = lax.broadcasted_iota(jnp.int32, (128, 256), 1)
    sum_low = same_group(wide_row // 96, wide_lane // 96)
    sum_mid = same_group((wide_row + 128) // 96, wide_lane // 96)
    sum_mid_last = same_group(
        (lax.broadcasted_iota(jnp.int32, (128, 128), 0) + 128) // 96, (lane_iota(128) + 256) // 96
    )
    sum_high = same_group((wide_row + 256) // 96, (wide_lane + 128) // 96)

    def masking(begin):
        return jnp.where(
            lane == begin, 1.0, jnp.where((lane == begin + 1) & early, 1.0, 0.0)
        )

    free = [lane >= 96, (lane >= 64) & (lane < 96), (lane >= 32) & (lane < 64), lane < 32]
    selects = [masking(begin) for begin in (96, 64, 32, 0)]
    for four in range(heads // 4):
        raw = [
            query[:, four * 384 + t * 128 : four * 384 + t * 128 + 128].astype(jnp.float32)
            for t in range(3)
        ]
        squares = [split_high_low(t * t) for t in raw]
        from_low = jnp.dot(squares[0], sum_low, preferred_element_type=jnp.float32)
        from_mid = jnp.dot(squares[1], sum_mid, preferred_element_type=jnp.float32)
        from_mid_last = jnp.dot(squares[1], sum_mid_last, preferred_element_type=jnp.float32)
        from_high = jnp.dot(squares[2], sum_high, preferred_element_type=jnp.float32)
        sums = [
            from_low[:, :128] + from_mid[:, :128],
            from_low[:, 128:] + from_mid[:, 128:] + from_high[:, :128],
            from_mid_last + from_high[:, 128:],
        ]
        turned = [
            turn_lanes(
                raw[t] * lax.rsqrt(sums[t] * (1.0 / 96) + eps) * gain_tiles[t], *turn_tiles[t]
            )
            for t in range(3)
        ]
        query_at = [
            turned[0],
            jnp.where(lane < 96, turned[1], turned[0]),
            jnp.where(lane < 64, turned[2], turned[1]),
            turned[2],
        ]
        for k in range(4):
            head = four * 4 + k
            out[head * rows : (head + 1) * rows, :] = jnp.where(
                free[k], selects[k], query_at[k]
            ).astype(jnp.bfloat16)


def attend_kernel(
    gathered,
    query,
    key_weight_turned,
    key_gain,
    cos_all,
    sin_all,
    value_weight_far,
    out_weight,
    out,
    out_weight_here,
    value_weight,
    latents,
    key_parts,
    keys,
    ropes,
    sums,
    arrivals,
):
    moves = start_moves(
        ((value_weight_far, value_weight), (out_weight, out_weight_here)), arrivals
    )
    own = lax.axis_index("sp")
    tokens = query.shape[0] // 16
    block = tokens + 16
    length = latents.shape[0]
    heads = key_weight_turned.shape[0] // 64
    scale = 96 ** (-0.5) * 1.4426950408889634
    half_gain = [key_gain[64:80, 0:1], key_gain[80:96, 0:1]]
    for device in range(length // tokens):
        at, here = device * block, slice(device * tokens, (device + 1) * tokens)
        latents[here, :] = gathered[at : at + tokens, :]
        first = gathered[at + tokens : at + block, 0:128].astype(jnp.float32)
        second = gathered[at + tokens : at + block, 128:256].astype(jnp.float32)
        sums[:, here] = jnp.sum(first * first + second * second, axis=0, keepdims=True)
        first, second = first * half_gain[0], second * half_gain[1]
        cos_part, sin_part = cos_all[:, here], sin_all[:, here]
        ropes[0:16, here] = first * cos_part - second * sin_part
        ropes[16:32, here] = second * cos_part + first * sin_part
    row = lax.broadcasted_iota(jnp.int32, (32, length), 0)
    key = lax.broadcasted_iota(jnp.int32, (32, length), 1)
    later = (row == 0) & (key >= (own + 1) * tokens)
    beside = (row == 1) & (key >= own * tokens + SPAN) & (key < (own + 1) * tokens)
    hidden = jnp.where(later | beside, -1e30, 0.0).astype(jnp.bfloat16)
    for k in range(4):
        keys[k, (96 * k + 96) % 128 : (96 * k + 96) % 128 + 32, :] = hidden
    for at in range(0, length, 256):
        key_parts[:, at : at + 256] = lax.dot_general(
            key_weight_turned[...],
            latents[at : at + 256, :],
            (((1,), (1,)), ((), ())),
            preferred_element_type=jnp.float32,
        ).astype(jnp.bfloat16)
    low_gain = jnp.broadcast_to(key_gain[0:64, 0:1], (64, 128))
    low_gain = jnp.concatenate([low_gain] * (length // 128), axis=1)

    def scores_of(head):
        part = key_parts[head * 64 : (head + 1) * 64, :].astype(jnp.float32)
        total = jnp.sum(part * part, axis=0, keepdims=True) + sums[...]
        inverse = lax.rsqrt(total * (1.0 / 96) + eps)
        part = (part * inverse * low_gain).astype(jnp.bfloat16)
        turned = (ropes[...] * inverse).astype(jnp.bfloat16)
        kind, begin = head % 4, (96 * head) % 128
        for piece, source in ((0, part[0:32]), (32, part[32:64]), (64, turned)):
            at = (begin + piece) % 128
            keys[kind, at : at + 32, :] = source
        return jnp.dot(
            query[head * tokens : (head + 1) * tokens, :],
            keys[kind],
            preferred_element_type=jnp.float32,
        )

    def fold(array, combine):
        parts = [array[:, at : at + 128] for at in range(0, array.shape[1], 128)]
        while len(parts) > 1:
            parts = [combine(*parts[at : at + 2]) for at in range(0, len(parts), 2)]
        return parts[0]

    lane = lane_iota(tokens)
    coming = scores_of(0)
    moves[0].wait()
    for head in range(heads):
        scores = coming
        if head + 1 < heads:
            coming = scores_of(head + 1)
        top = jnp.max(fold(scores, jnp.maximum), axis=-1, keepdims=True)
        raised = jnp.exp2(scores * scale - top * scale)
        row_sum = jnp.sum(fold(raised, jnp.add), axis=-1, keepdims=True)
        mixed = jnp.dot(
            raised.astype(jnp.bfloat16), latents[...], preferred_element_type=jnp.float32
        )
        mixed = (mixed * (1.0 / row_sum)).astype(jnp.bfloat16)
        pair = (head // 2) * 128
        both = jnp.dot(
            mixed, value_weight[:, pair : pair + 128], preferred_element_type=jnp.float32
        )
        if head % 2:
            out[:, pair : pair + 128] = jnp.where(lane < 64, before, both).astype(jnp.bfloat16)
        else:
            before = both
    moves[1].wait()


def mix_kernel(heads_out, residual, mix_gain, out_weight, ffn_gain, spread, stream_out, outgoing):
    width = residual.shape[1]
    wide = heads_out[...].astype(jnp.float32)
    mixed_in = (wide * inverse_rms(wide, wide.shape[1]) * mix_gain[...]).astype(jnp.bfloat16)
    stream = residual[...].astype(jnp.float32) + jnp.dot(
        mixed_in, out_weight[...], preferred_element_type=jnp.float32
    )
    stream_out[...] = stream
    normed = (stream * inverse_rms(stream, width) * ffn_gain[...]).astype(jnp.bfloat16)
    stacked = jnp.concatenate([normed[:, : width // 2], normed[:, width // 2 :]], axis=0)
    outgoing[...] = jnp.dot(
        spread[...], stacked, preferred_element_type=jnp.float32
    ).astype(jnp.bfloat16)


def unstack(blocks, rows_out):
    pairs, width = blocks.shape[0] // 16, blocks.shape[1]
    view = blocks[...].astype(jnp.float32).reshape(pairs, 2, 8, width)
    one, two = view[:, 0], view[:, 1]
    upper = lax.broadcasted_iota(jnp.int32, (pairs, 8, width), 1) < 4
    low = jnp.where(upper, one, pltpu.roll(two, 4, 1))
    high = jnp.where(upper, pltpu.roll(one, 4, 1), two)
    rows_out[:, 0:width] = low.reshape(pairs * 8, width).astype(jnp.bfloat16)
    rows_out[:, width : 2 * width] = high.reshape(pairs * 8, width).astype(jnp.bfloat16)


def expert_kernel(arrived, gate_weight, up_weight, down_weight, out, rows_in):
    unstack(arrived, rows_in)
    gate_act = jnp.dot(rows_in[...], gate_weight[0], preferred_element_type=jnp.float32)
    upward = jnp.dot(rows_in[...], up_weight[0], preferred_element_type=jnp.float32)
    hidden = (jax.nn.silu(gate_act) * upward).astype(jnp.bfloat16)
    expert_out = jnp.dot(hidden, down_weight[0], preferred_element_type=jnp.float32)
    rows, width = expert_out.shape
    width = width // 2
    low = expert_out[:, :width].reshape(rows // 8, 8, width)
    high = expert_out[:, width:].reshape(rows // 8, 8, width)
    upper = lax.broadcasted_iota(jnp.int32, (rows // 8, 8, width), 1) < 4
    one = jnp.where(upper, low, pltpu.roll(high, 4, 1))
    two = jnp.where(upper, pltpu.roll(low, 4, 1), high)
    both = jnp.concatenate([one[:, None], two[:, None]], axis=1)
    out[...] = both.reshape(rows * 2, width).astype(jnp.bfloat16)


def combine_kernel(returned, gather, stream, route_weight, out, rows_back):
    unstack(returned, rows_back)
    tokens = stream.shape[0]
    picked = jnp.dot(gather[...], rows_back[...], preferred_element_type=jnp.float32)
    routed = route_weight[:, 0:1] * picked[:tokens] + route_weight[:, 1:2] * picked[tokens:]
    out[...] = (stream[...] + routed).astype(jnp.bfloat16)


VMEM = pl.BlockSpec(memory_space=pltpu.VMEM)
HBM = pl.BlockSpec(memory_space=pltpu.HBM)


def call(body, in_specs, out_shapes, mib, scratch=(), name=None):
    many = isinstance(out_shapes, tuple)
    run = pl.pallas_call(
        body,
        in_specs=in_specs,
        out_shape=out_shapes,
        out_specs=tuple(VMEM for _ in out_shapes) if many else VMEM,
        scratch_shapes=list(scratch),
        compiler_params=pltpu.CompilerParams(vmem_limit_bytes=mib * 2**20),
        name=name,
    )

    def placed(*operands):
        return run(
            *(
                pltpu.with_memory_space_constraint(x, pltpu.HBM) if spec is HBM else x
                for spec, x in zip(in_specs, operands)
            )
        )

    return placed


def per_device(
    residual,
    query,
    latent,
    rope_key,
    latent_gain,
    query_gain,
    key_gain,
    key_weight,
    value_weight,
    mix_gain,
    out_weight,
    ffn_gain,
    expert_choice,
    group_prob,
    expert_prob,
    gate_weight,
    up_weight,
    down_weight,
):
    tokens = residual.shape[1]
    width = residual.shape[2]
    devices = lax.axis_size("sp")
    sequence = tokens * devices
    shape = jax.ShapeDtypeStruct
    half, full = jnp.bfloat16, jnp.float32
    block = tokens + 16
    packed = call(
        pack_kernel,
        [HBM] * 3,
        shape((devices * block, 256), half),
        6,
        scratch=(
            pltpu.VMEM(latent.shape[1:], half),
            pltpu.VMEM(rope_key.shape[:0:-1], half),
            pltpu.VMEM((1,) + latent_gain.shape, full),
            pltpu.SemaphoreType.DMA((3,)),
        ),
        name="pack",
    )(latent[0], rope_key[0].T, latent_gain[None])
    gathered = lax.all_to_all(packed, "sp", split_axis=0, concat_axis=0, tiled=True)
    own = angles(lax.axis_index("sp") * tokens, tokens, rope_key.shape[2])
    every = angles(0, sequence, rope_key.shape[2]).T
    (
        queries,
        key_weight_turned,
        spread,
        gather,
        route_weight,
    ) = call(
        query_kernel,
        [HBM] * 3 + [VMEM] * 5,
        (
            shape((16 * tokens, 128), half),
            shape(key_weight.shape[::-1], half),
            shape((1024, 256), half),
            shape((256, 512), half),
            shape((tokens, 2), full),
        ),
        22,
        scratch=(
            pltpu.VMEM(query.shape[1:], half),
            pltpu.VMEM((1,) + query_gain.shape, full),
            pltpu.VMEM(key_weight.shape, half),
            pltpu.SemaphoreType.DMA((3,)),
            pltpu.VMEM((8, 128), full),
            pltpu.VMEM((tokens, 384), full),
        ),
        name="query",
    )(
        query[0],
        query_gain[None],
        key_weight,
        jnp.cos(own),
        jnp.sin(own),
        expert_choice[0].T,
        group_prob,
        expert_prob[0].T,
    )
    heads_out, out_weight = call(
        attend_kernel,
        [VMEM] * 6 + [HBM] * 2,
        (shape((tokens, 1024), half), shape(out_weight.shape, half)),
        30,
        scratch=(
            pltpu.VMEM(value_weight.shape, half),
            pltpu.VMEM((sequence, 256), half),
            pltpu.VMEM((1024, sequence), half),
            pltpu.VMEM((4, 128, sequence), half),
            pltpu.VMEM((32, sequence), full),
            pltpu.VMEM((1, sequence), full),
            pltpu.SemaphoreType.DMA((2,)),
        ),
        name="attend",
    )(
        gathered,
        queries,
        key_weight_turned,
        key_gain[:, None],
        jnp.cos(every),
        jnp.sin(every),
        value_weight,
        out_weight,
    )
    stream, outgoing = call(
        mix_kernel,
        [VMEM] * 6,
        (shape((tokens, width), full), shape((1024, 1024), half)),
        16,
        name="mix",
    )(heads_out, residual[0], mix_gain[None], out_weight, ffn_gain[None], spread)
    arrived = lax.all_to_all(outgoing, ("sp", "dp"), split_axis=0, concat_axis=0, tiled=True)
    answers = call(
        expert_kernel,
        [VMEM] * 4,
        shape((1024, 1024), half),
        20,
        scratch=(pltpu.VMEM((512, width), half),),
        name="expert",
    )(arrived, gate_weight, up_weight, down_weight)
    returned = lax.all_to_all(answers, ("sp", "dp"), split_axis=0, concat_axis=0, tiled=True)
    return call(
        combine_kernel,
        [VMEM] * 4,
        shape((tokens, width), half),
        14,
        scratch=(pltpu.VMEM((512, width), half),),
        name="combine",
    )(returned, gather, stream, route_weight)[None]


def solution(mesh):
    return jax.shard_map(
        per_device,
        mesh=mesh,
        in_specs=(
            P("dp", "sp", None),
            P("dp", "sp", None),
            P("dp", "sp", None),
            P("dp", "sp", None),
            P(),
            P(),
            P(),
            P(),
            P(),
            P(),
            P(),
            P(),
            P("dp", "sp", None),
            P("dp", "sp"),
            P("dp", "sp", None),
            P(("sp", "dp"), None, None),
            P(("sp", "dp"), None, None),
            P(("sp", "dp"), None, None),
        ),
        out_specs=P("dp", "sp", None),
        check_vma=False,
    )
```

time: 149 us -> 120 us (0.81)
  waiting for transfers between devices: 34 us -> 13.7 us
  Pallas kernels: 34.7 us -> 24.2 us
  blocking collectives: 63.7 us -> 72.4 us
  local copies, waits for them, and re-layouts: 5.21 us -> 0.15 us
    all_to_all x2 -> x1, waiting for transfers between devices: 34 us -> 13.7 us  [per_device(): lax.all_to_all(packed, 'sp', split_axis=0, concat_axis=0, tiled=True)]
    pallas_call x6, Pallas kernels: 34.7 us -> 24.2 us  [placed(): run(*(pltpu.with_memory_space_constraint(x, pltpu.HBM) if spec is HBM els...]
    all_to_all x1, blocking collectives: 24.9 us -> 34.4 us  [per_device(): lax.all_to_all(answers, ('sp', 'dp'), split_axis=0, concat_axis=0, tiled=...]
    unnamed x13 -> x20, local copies, waits for them, and re-layouts: 4.3 us -> 0.05 us
    all_to_all x2 -> x1, starting transfers between devices: 8.07 us -> 8.6 us  [per_device(): lax.all_to_all(packed, 'sp', split_axis=0, concat_axis=0, tiled=True)]
  transfers between devices with their start and end apart: 2 -> 1, of which waited for: 2 -> 1; matrix products, arithmetic and copies ran while one was open for 1% -> 1% of each run, Pallas kernels for 2% -> 2%
where the time goes in v5:
time: 120 us
  blocking collectives  72.4 us (60%)
  Pallas kernels  24.2 us (20%)
  waiting for transfers between devices  13.7 us (11%)
  starting transfers between devices  8.6 us (7%)
    all_to_all x1, blocking collectives, per_device(): lax.all_to_all(outgoing, ('sp', 'dp'), split_axis=0, concat_axis=0, tiled...  38 us
    all_to_all x1, blocking collectives, per_device(): lax.all_to_all(answers, ('sp', 'dp'), split_axis=0, concat_axis=0, tiled=...  34.4 us
    pallas_call x6, Pallas kernels, placed(): run(*(pltpu.with_memory_space_constraint(x, pltpu.HBM) if spec is HBM els...  24.2 us
    all_to_all x1, waiting for transfers between devices, per_device(): lax.all_to_all(packed, 'sp', split_axis=0, concat_axis=0, tiled=True)  13.7 us
    all_to_all x1, starting transfers between devices, per_device(): lax.all_to_all(packed, 'sp', split_axis=0, concat_axis=0, tiled=True)  8.6 us
  transfers between devices with their start and end apart: 1, of which 1 were waited for; matrix products, arithmetic and copies ran while one was open for 1% of the time, Pallas kernels for 2%

profile of v5, /device:TPU:1, one launch (start us, length us, event | category | flops | bytes accessed | tf_op | source)
XLA Modules:
  0.0 120.1 jit_solution(5148640877643681477)
XLA Ops:
  0.0 0.0 copy-start.6
  0.0 2.1 %pack.1 = bf16[2304,256]{1,0:T(8,128)(2,1)} custom-call(bf16[128,256]{1,0:T(8,128)(2,1)} %bitcast.35, bf16[32,128]{1,0:T(8,128)(2,1)} %bitcast.36, f32[1,256]{1,0:T(1,128)} %bitcast.37), custom_call_target="tpu_custom_call" | custom-call | tf_op jit(solution)/shard_map/pack/pallas_call | solution.py:396
  2.2 8.6 %all-to-all-start = ((bf16[16,144,256]{2,1,0:T(8,128)(2,1)}), bf16[16,144,256]{2,1,0:T(8,128)(2,1)S(1)}, u32[]{:S(2)}, u32[]{:S(2)}) async-start(bf16[16,144,256]{2,1,0:T(8,128)(2,1)} %bitcast.4), calls=%async_computation | async-start | bytes 2359296 | tf_op jit(solution)/shard_map/all_to_all | solution.py:446
  10.8 0.0 copy-done.9
  10.8 0.1 copy.21.key_gain
  10.9 0.3 multiply_sine_fusion.1
  11.2 0.0 copy-done.7
  11.2 0.0 copy-done.8
  11.2 0.0 copy-done.6
  11.2 2.7 %query.1 = (bf16[2048,128]{1,0:T(8,128)(2,1)S(1)}, bf16[1024,256]{1,0:T(8,128)(2,1)S(1)}, bf16[1024,256]{1,0:T(8,128)(2,1)S(1)}, bf16[256,512]{1,0:T(8,128)(2,1)S(1)}, f32[128,2]{1,0:T(8,128)S(1)}) custom-call(bf16[128,1536]{1,0:T(8,128)(2,1)} %bitcast.34, f32[1,96]{1,0:T(1,128)} %bitcast.38, bf16[256,1024]{1,0:T(8,128)(2,1)} %key_weight.1, ...), custom_call_target="tpu_custom_call" | custom-call | tf_op jit(solution)/shard_map/query/pallas_call | solution.py:396
  13.9 0.5 multiply_sine_fusion
  14.5 13.7 %all-to-all-done = bf16[16,144,256]{2,1,0:T(8,128)(2,1)S(1)} async-done(((bf16[16,144,256]{2,1,0:T(8,128)(2,1)}), bf16[16,144,256]{2,1,0:T(8,128)(2,1)S(1)}, u32[]{:S(2)}, u32[]{:S(2)}) %all-to-all-start) | async-done | bytes 1179680 | tf_op jit(solution)/shard_map/all_to_all | solution.py:446
  28.2 12.5 %attend.1 = (bf16[128,1024]{1,0:T(8,128)(2,1)S(1)}, bf16[1024,2048]{1,0:T(8,128)(2,1)S(1)}) custom-call(bf16[2304,256]{1,0:T(8,128)(2,1)S(1)} %bitcast.27, bf16[2048,128]{1,0:T(8,128)(2,1)S(1)} %get-tuple-element.14.query, bf16[1024,256]{1,0:T(8,128)(2,1)S(1)} %get-tuple-element.15.key_weight_turned, f32[96,1]{1,0:T(8,128)S(1)} %copy.21.key_gain, ...), custom_call_target="tpu_custom_call" | custom-call | tf_op jit(solution)/shard_map/attend/pallas_call | solution.py:396
  40.7 0.0 copy-done.3
  40.7 0.0 copy-done.4
  40.7 0.0 copy-start.2
  40.7 1.6 %mix.1 = (f32[128,2048]{1,0:T(8,128)S(1)}, bf16[1024,1024]{1,0:T(8,128)(2,1)S(1)}) custom-call(bf16[128,1024]{1,0:T(8,128)(2,1)S(1)} %get-tuple-element.16.heads_out, bf16[128,2048]{1,0:T(8,128)(2,1)S(1)} %bitcast.29, f32[1,1024]{1,0:T(1,128)S(1)} %bitcast.31, bf16[1024,2048]{1,0:T(8,128)(2,1)S(1)} %get-tuple-element.17.out_weight, f32[1,2048]{1,0:T(1,128)S(1)} %bitcast.30, ...), custom_call_target="tpu_custom_call" | custom-call | tf_op jit(solution)/shard_map/mix/pallas_call | solution.py:396
  42.4 0.0 copy-start
  42.4 0.0 copy-start.1
  42.4 38.0 %all_to_all.33 = bf16[128,8,1024]{2,1,0:T(8,128)(2,1)S(1)} all-to-all(bf16[128,8,1024]{2,1,0:T(8,128)(2,1)S(1)} %bitcast.28), channel_id=1, replica_groups=mesh['sp'=16,'dp'=8] {'sp','dp'}, dimensions={0} | all-to-all | bytes 4194304 | tf_op jit(solution)/shard_map/all_to_all | solution.py:517
  80.4 0.0 copy-done
  80.4 3.5 %expert.1 = bf16[1024,1024]{1,0:T(8,128)(2,1)S(1)} custom-call(bf16[1024,1024]{1,0:T(8,128)(2,1)S(1)} %bitcast.24, bf16[1,2048,512]{2,1,0:T(8,128)(2,1)S(1)} %copy-done, bf16[1,2048,512]{2,1,0:T(8,128)(2,1)S(1)} %copy-done.1, bf16[1,512,2048]{2,1,0:T(8,128)(2,1)S(1)} %copy-done.2), custom_call_target="tpu_custom_call" | custom-call | tf_op jit(solution)/shard_map/expert/pallas_call | solution.py:396
  83.9 34.4 %all_to_all.34 = bf16[128,8,1024]{2,1,0:T(8,128)(2,1)S(1)} all-to-all(bf16[128,8,1024]{2,1,0:T(8,128)(2,1)S(1)} %bitcast.25), channel_id=1, replica_groups=mesh['sp'=16,'dp'=8] {'sp','dp'}, dimensions={0} | all-to-all | bytes 4194304 | tf_op jit(solution)/shard_map/all_to_all | solution.py:526
  118.3 1.8 %combine.1 = bf16[128,2048]{1,0:T(8,128)(2,1)} custom-call(bf16[1024,1024]{1,0:T(8,128)(2,1)S(1)} %bitcast.26, bf16[256,512]{1,0:T(8,128)(2,1)S(1)} %get-tuple-element.20.gather, f32[128,2048]{1,0:T(8,128)S(1)} %get-tuple-element.21.stream, f32[128,2]{1,0:T(8,128)S(1)} %get-tuple-element.22.route_weight), custom_call_target="tpu_custom_call" | custom-call | tf_op jit(solution)/shard_map/combine/pallas_call | solution.py:396
  (12 shorter events, 0.0 us)
Async XLA Ops:
  0.0 10.8 %copy-start.9 = (f32[96]{0:T(128)S(1)}, f32[96]{0:T(128)}, u32[]{:S(2)}) copy-start(f32[96]{0:T(128)} %param.24) | copy-start | bytes 1156
  0.0 11.2 %copy-start.7 = (f32[1,128,2]{1,2,0:T(2,128)S(1)}, f32[1,128,2]{1,2,0:T(2,128)}, u32[]{:S(2)}) copy-start(f32[1,128,2]{1,2,0:T(2,128)} %param.32) | copy-start | bytes 3076
  0.0 11.2 %copy-start.8 = (f32[1,128]{1,0:T(1,128)S(1)}, f32[1,128]{1,0:T(1,128)}, u32[]{:S(2)}) copy-start(f32[1,128]{1,0:T(1,128)} %group_prob.1) | copy-start | bytes 1540
  0.0 11.2 %copy-start.6 = (s32[1,128,2]{1,2,0:T(2,128)S(1)}, s32[1,128,2]{1,2,0:T(2,128)}, u32[]{:S(2)}) copy-start(s32[1,128,2]{1,2,0:T(2,128)} %param.30) | copy-start | bytes 3076
  2.2 26.1 %all-to-all-start = ((bf16[16,144,256]{2,1,0:T(8,128)(2,1)}), bf16[16,144,256]{2,1,0:T(8,128)(2,1)S(1)}, u32[]{:S(2)}, u32[]{:S(2)}) async-start(bf16[16,144,256]{2,1,0:T(8,128)(2,1)} %bitcast.4), calls=%async_computation | async-start | bytes 2359296 | tf_op jit(solution)/shard_map/all_to_all | solution.py:446
  28.2 12.5 %copy-start.3 = (bf16[1,128,2048]{2,1,0:T(8,128)(2,1)S(1)}, bf16[1,128,2048]{2,1,0:T(8,128)(2,1)}, u32[]{:S(2)}) copy-start(bf16[1,128,2048]{2,1,0:T(8,128)(2,1)} %param.18) | copy-start | bytes 1572868
  28.2 12.5 %copy-start.4 = (f32[2048]{0:T(1024)S(1)}, f32[2048]{0:T(1024)}, u32[]{:S(2)}) copy-start(f32[2048]{0:T(1024)} %param.29) | copy-start | bytes 24580
  28.2 12.5 %copy-start.5 = (f32[1024]{0:T(1024)S(1)}, f32[1024]{0:T(1024)}, u32[]{:S(2)}) copy-start(f32[1024]{0:T(1024)} %param.27) | copy-start | bytes 12292
  40.7 39.7 %copy-start.2 = (bf16[1,512,2048]{2,1,0:T(8,128)(2,1)S(1)}, bf16[1,512,2048]{2,1,0:T(8,128)(2,1)}, u32[]{:S(2)}) copy-start(bf16[1,512,2048]{2,1,0:T(8,128)(2,1)} %down_weight.1) | copy-start | bytes 6291460
  42.4 38.0 %copy-start = (bf16[1,2048,512]{2,1,0:T(8,128)(2,1)S(1)}, bf16[1,2048,512]{2,1,0:T(8,128)(2,1)}, u32[]{:S(2)}) copy-start(bf16[1,2048,512]{2,1,0:T(8,128)(2,1)} %gate_weight.1) | copy-start | bytes 6291460
  42.4 38.0 %copy-start.1 = (bf16[1,2048,512]{2,1,0:T(8,128)(2,1)S(1)}, bf16[1,2048,512]{2,1,0:T(8,128)(2,1)}, u32[]{:S(2)}) copy-start(bf16[1,2048,512]{2,1,0:T(8,128)(2,1)} %up_weight.1) | copy-start | bytes 6291460

commit v6 on v5

--- a/solution.py
+++ b/solution.py
@@ -226,6 +226,7 @@
     gathered,
     query,
     key_weight_turned,
+    query_gain,
     key_gain,
     cos_all,
     sin_all,
@@ -239,6 +240,7 @@
     keys,
     ropes,
     sums,
+    weights,
     arrivals,
 ):
     moves = start_moves(
@@ -278,18 +280,18 @@
     low_gain = jnp.broadcast_to(key_gain[0:64, 0:1], (64, 128))
     low_gain = jnp.concatenate([low_gain] * (length // 128), axis=1)
 
-    def scores_of(head):
-        part = key_parts[head * 64 : (head + 1) * 64, :].astype(jnp.float32)
+    def scores_of(head, kind):
+        part = key_parts[pl.ds(head * 64, 64), :].astype(jnp.float32)
         total = jnp.sum(part * part, axis=0, keepdims=True) + sums[...]
         inverse = lax.rsqrt(total * (1.0 / 96) + eps)
         part = (part * inverse * low_gain).astype(jnp.bfloat16)
         turned = (ropes[...] * inverse).astype(jnp.bfloat16)
-        kind, begin = head % 4, (96 * head) % 128
+        begin = (96 * kind) % 128
         for piece, source in ((0, part[0:32]), (32, part[32:64]), (64, turned)):
             at = (begin + piece) % 128
             keys[kind, at : at + 32, :] = source
         return jnp.dot(
-            query[head * tokens : (head + 1) * tokens, :],
+            query[pl.ds(head * tokens, tokens), :],
             keys[kind],
             preferred_element_type=jnp.float32,
         )
@@ -301,27 +303,63 @@
         return parts[0]
 
     lane = lane_iota(tokens)
-    coming = scores_of(0)
+
+    def finish(first_head, count, buffer, row_sums):
+        mixed = jnp.dot(
+            weights[buffer, 0 : count * tokens, :], latents[...], preferred_element_type=jnp.float32
+        )
+        for two in range(0, count, 2):
+            rows = [
+                mixed[(two + odd) * tokens : (two + odd + 1) * tokens] * (1.0 / row_sums[two + odd])
+                for odd in range(2)
+            ]
+            at = first_head * 64 + two * 64
+            at = at if isinstance(at, int) else pl.multiple_of(at, 128)
+            both = jnp.dot(
+                jnp.concatenate(rows, axis=0).astype(jnp.bfloat16),
+                value_weight[:, pl.ds(at, 128)],
+                preferred_element_type=jnp.float32,
+            )
+            out[:, pl.ds(at, 128)] = jnp.where(lane < 64, both[:tokens], both[tokens:]).astype(
+                jnp.bfloat16
+            )
+
     moves[0].wait()
-    for head in range(heads):
-        scores = coming
-        if head + 1 < heads:
-            coming = scores_of(head + 1)
-        top = jnp.max(fold(scores, jnp.maximum), axis=-1, keepdims=True)
-        raised = jnp.exp2(scores * scale - top * scale)
-        row_sum = jnp.sum(fold(raised, jnp.add), axis=-1, keepdims=True)
-        mixed = jnp.dot(
-            raised.astype(jnp.bfloat16), latents[...], preferred_element_type=jnp.float32
-        )
-        mixed = (mixed * (1.0 / row_sum)).astype(jnp.bfloat16)
-        pair = (head // 2) * 128
-        both = jnp.dot(
-            mixed, value_weight[:, pair : pair + 128], preferred_element_type=jnp.float32
-        )
-        if head % 2:
-            out[:, pair : pair + 128] = jnp.where(lane < 64, before, both).astype(jnp.bfloat16)
-        else:
-            before = both
+    bound = 14.2 * jnp.max(jnp.abs(query_gain[...])) * jnp.max(jnp.abs(key_gain[...]))
+    narrow = bound < 100.0
+
+    @pl.when(narrow)
+    def _():
+        waiting = None
+        for first_head in range(0, heads, 2):
+            buffer = (first_head // 2) % 2
+            row_sums = []
+            for k in range(2):
+                raised = jnp.exp2(scores_of(first_head + k, (first_head + k) % 4) * scale)
+                row_sums.append(jnp.sum(fold(raised, jnp.add), axis=-1, keepdims=True))
+                weights[buffer, k * tokens : (k + 1) * tokens, :] = raised.astype(jnp.bfloat16)
+            if waiting is not None:
+                finish(*waiting)
+            waiting = (first_head, 2, buffer, row_sums)
+        finish(*waiting)
+
+    @pl.when(jnp.logical_not(narrow))
+    def _():
+        def four_heads(step, carry):
+            row_sums = []
+            for kind in range(4):
+                scores = scores_of(step * 4 + kind, kind)
+                top = jnp.max(fold(scores, jnp.maximum), axis=-1, keepdims=True)
+                raised = jnp.exp2((scores - top) * scale)
+                row_sums.append(jnp.sum(fold(raised, jnp.add), axis=-1, keepdims=True))
+                at = (kind % 2) * tokens
+                weights[kind // 2, at : at + tokens, :] = raised.astype(jnp.bfloat16)
+                if kind % 2:
+                    finish(step * 4 + kind - 1, 2, kind // 2, row_sums[kind - 1 :])
+            return carry
+
+        lax.fori_loop(0, heads // 4, four_heads, 0)
+
     moves[1].wait()
 
 
@@ -484,7 +522,7 @@
     )
     heads_out, out_weight = call(
         attend_kernel,
-        [VMEM] * 6 + [HBM] * 2,
+        [VMEM] * 7 + [HBM] * 2,
         (shape((tokens, 1024), half), shape(out_weight.shape, half)),
         30,
         scratch=(
@@ -494,6 +532,7 @@
             pltpu.VMEM((4, 128, sequence), half),
             pltpu.VMEM((32, sequence), full),
             pltpu.VMEM((1, sequence), full),
+            pltpu.VMEM((2, 2 * tokens, sequence), half),
             pltpu.SemaphoreType.DMA((2,)),
         ),
         name="attend",
@@ -501,6 +540,7 @@
         gathered,
         queries,
         key_weight_turned,
+        query_gain[None],
         key_gain[:, None],
         jnp.cos(every),
         jnp.sin(every),

time: 120 us -> 121 us (level)
  no operation moved by 1% of the time
where the time goes in v6:
time: 121 us; the launch traced here: 120 us
  blocking collectives  72.4 us (60%)
  Pallas kernels  24.4 us (20%)
  waiting for transfers between devices  13.7 us (11%)
  starting transfers between devices  8.6 us (7%)
    all_to_all x1, blocking collectives, per_device(): lax.all_to_all(outgoing, ('sp', 'dp'), split_axis=0, concat_axis=0, tiled...  38 us
    all_to_all x1, blocking collectives, per_device(): lax.all_to_all(answers, ('sp', 'dp'), split_axis=0, concat_axis=0, tiled=...  34.4 us
    pallas_call x6, Pallas kernels, placed(): run(*(pltpu.with_memory_space_constraint(x, pltpu.HBM) if spec is HBM els...  24.4 us
    all_to_all x1, waiting for transfers between devices, per_device(): lax.all_to_all(packed, 'sp', split_axis=0, concat_axis=0, tiled=True)  13.7 us
    all_to_all x1, starting transfers between devices, per_device(): lax.all_to_all(packed, 'sp', split_axis=0, concat_axis=0, tiled=True)  8.6 us
  transfers between devices with their start and end apart: 1, of which 1 were waited for; matrix products, arithmetic and copies ran while one was open for 1% of the time, Pallas kernels for 2%

profile of v6, /device:TPU:1, one launch (start us, length us, event | category | flops | bytes accessed | tf_op | source)
XLA Modules:
  0.0 120.3 jit_solution(4699985321666021111)
XLA Ops:
  0.0 2.1 %pack.1 = bf16[2304,256]{1,0:T(8,128)(2,1)} custom-call(bf16[128,256]{1,0:T(8,128)(2,1)} %bitcast.37, bf16[32,128]{1,0:T(8,128)(2,1)} %bitcast.38, f32[1,256]{1,0:T(1,128)} %bitcast.39), custom_call_target="tpu_custom_call" | custom-call | tf_op jit(solution)/shard_map/pack/pallas_call | solution.py:434
  2.2 0.0 copy-start.6
  2.2 8.6 %all-to-all-start = ((bf16[16,144,256]{2,1,0:T(8,128)(2,1)}), bf16[16,144,256]{2,1,0:T(8,128)(2,1)S(1)}, u32[]{:S(2)}, u32[]{:S(2)}) async-start(bf16[16,144,256]{2,1,0:T(8,128)(2,1)} %bitcast.4), calls=%async_computation | async-start | bytes 2359296 | tf_op jit(solution)/shard_map/all_to_all | solution.py:484
  10.8 0.1 copy.21.key_gain
  10.9 0.3 multiply_sine_fusion.1
  11.2 0.0 copy-done.8
  11.3 0.0 copy-done.9
  11.3 0.0 copy-done.7
  11.3 2.7 %query.1 = (bf16[2048,128]{1,0:T(8,128)(2,1)S(1)}, bf16[1024,256]{1,0:T(8,128)(2,1)S(1)}, bf16[1024,256]{1,0:T(8,128)(2,1)S(1)}, bf16[256,512]{1,0:T(8,128)(2,1)S(1)}, f32[128,2]{1,0:T(8,128)S(1)}) custom-call(bf16[128,1536]{1,0:T(8,128)(2,1)} %bitcast.36, f32[1,96]{1,0:T(1,128)} %bitcast.32, bf16[256,1024]{1,0:T(8,128)(2,1)} %key_weight.1, ...), custom_call_target="tpu_custom_call" | custom-call | tf_op jit(solution)/shard_map/query/pallas_call | solution.py:434
  14.0 0.5 multiply_sine_fusion
  14.5 13.7 %all-to-all-done = bf16[16,144,256]{2,1,0:T(8,128)(2,1)S(1)} async-done(((bf16[16,144,256]{2,1,0:T(8,128)(2,1)}), bf16[16,144,256]{2,1,0:T(8,128)(2,1)S(1)}, u32[]{:S(2)}, u32[]{:S(2)}) %all-to-all-start) | async-done | bytes 1179680 | tf_op jit(solution)/shard_map/all_to_all | solution.py:484
  28.2 0.0 copy-done.6
  28.2 12.7 %attend.1 = (bf16[128,1024]{1,0:T(8,128)(2,1)S(1)}, bf16[1024,2048]{1,0:T(8,128)(2,1)S(1)}) custom-call(bf16[2304,256]{1,0:T(8,128)(2,1)S(1)} %bitcast.27, bf16[2048,128]{1,0:T(8,128)(2,1)S(1)} %get-tuple-element.14.query, bf16[1024,256]{1,0:T(8,128)(2,1)S(1)} %get-tuple-element.15.key_weight_turned, f32[1,96]{1,0:T(1,128)S(1)} %bitcast.33, ...), custom_call_target="tpu_custom_call" | custom-call | tf_op jit(solution)/shard_map/attend/pallas_call | solution.py:434
  41.0 0.0 copy-done.3
  41.0 0.0 copy-done.4
  41.0 0.0 copy-done.5
  41.0 0.0 copy-start.2
  41.0 1.6 %mix.1 = (f32[128,2048]{1,0:T(8,128)S(1)}, bf16[1024,1024]{1,0:T(8,128)(2,1)S(1)}) custom-call(bf16[128,1024]{1,0:T(8,128)(2,1)S(1)} %get-tuple-element.16.heads_out, bf16[128,2048]{1,0:T(8,128)(2,1)S(1)} %bitcast.29, f32[1,1024]{1,0:T(1,128)S(1)} %bitcast.31, bf16[1024,2048]{1,0:T(8,128)(2,1)S(1)} %get-tuple-element.17.out_weight, f32[1,2048]{1,0:T(1,128)S(1)} %bitcast.30, ...), custom_call_target="tpu_custom_call" | custom-call | tf_op jit(solution)/shard_map/mix/pallas_call | solution.py:434
  42.6 0.0 copy-start
  42.7 0.0 copy-start.1
  42.7 38.0 %all_to_all.33 = bf16[128,8,1024]{2,1,0:T(8,128)(2,1)S(1)} all-to-all(bf16[128,8,1024]{2,1,0:T(8,128)(2,1)S(1)} %bitcast.28), channel_id=1, replica_groups=mesh['sp'=16,'dp'=8] {'sp','dp'}, dimensions={0} | all-to-all | bytes 4194304 | tf_op jit(solution)/shard_map/all_to_all | solution.py:557
  80.7 3.5 %expert.1 = bf16[1024,1024]{1,0:T(8,128)(2,1)S(1)} custom-call(bf16[1024,1024]{1,0:T(8,128)(2,1)S(1)} %bitcast.24, bf16[1,2048,512]{2,1,0:T(8,128)(2,1)S(1)} %copy-done, bf16[1,2048,512]{2,1,0:T(8,128)(2,1)S(1)} %copy-done.1, bf16[1,512,2048]{2,1,0:T(8,128)(2,1)S(1)} %copy-done.2), custom_call_target="tpu_custom_call" | custom-call | tf_op jit(solution)/shard_map/expert/pallas_call | solution.py:434
  84.2 34.4 %all_to_all.34 = bf16[128,8,1024]{2,1,0:T(8,128)(2,1)S(1)} all-to-all(bf16[128,8,1024]{2,1,0:T(8,128)(2,1)S(1)} %bitcast.25), channel_id=1, replica_groups=mesh['sp'=16,'dp'=8] {'sp','dp'}, dimensions={0} | all-to-all | bytes 4194304 | tf_op jit(solution)/shard_map/all_to_all | solution.py:566
  118.6 1.8 %combine.1 = bf16[128,2048]{1,0:T(8,128)(2,1)} custom-call(bf16[1024,1024]{1,0:T(8,128)(2,1)S(1)} %bitcast.26, bf16[256,512]{1,0:T(8,128)(2,1)S(1)} %get-tuple-element.20.gather, f32[128,2048]{1,0:T(8,128)S(1)} %get-tuple-element.21.stream, f32[128,2]{1,0:T(8,128)S(1)} %get-tuple-element.22.route_weight), custom_call_target="tpu_custom_call" | custom-call | tf_op jit(solution)/shard_map/combine/pallas_call | solution.py:434
  (14 shorter events, 0.0 us)
Async XLA Ops:
  0.0 10.8 %copy-start.10 = (f32[96]{0:T(128)S(1)}, f32[96]{0:T(128)}, u32[]{:S(2)}) copy-start(f32[96]{0:T(128)} %param.24) | copy-start | bytes 1156
  0.0 11.2 %copy-start.8 = (f32[1,128,2]{1,2,0:T(2,128)S(1)}, f32[1,128,2]{1,2,0:T(2,128)}, u32[]{:S(2)}) copy-start(f32[1,128,2]{1,2,0:T(2,128)} %param.32) | copy-start | bytes 3076
  0.0 11.2 %copy-start.9 = (f32[1,128]{1,0:T(1,128)S(1)}, f32[1,128]{1,0:T(1,128)}, u32[]{:S(2)}) copy-start(f32[1,128]{1,0:T(1,128)} %group_prob.1) | copy-start | bytes 1540
  0.0 11.3 %copy-start.7 = (s32[1,128,2]{1,2,0:T(2,128)S(1)}, s32[1,128,2]{1,2,0:T(2,128)}, u32[]{:S(2)}) copy-start(s32[1,128,2]{1,2,0:T(2,128)} %param.30) | copy-start | bytes 3076
  2.2 26.1 %copy-start.6 = (f32[96]{0:T(128)S(1)}, f32[96]{0:T(128)}, u32[]{:S(2)}) copy-start(f32[96]{0:T(128)} %param.23) | copy-start | bytes 1156
  2.2 26.1 %all-to-all-start = ((bf16[16,144,256]{2,1,0:T(8,128)(2,1)}), bf16[16,144,256]{2,1,0:T(8,128)(2,1)S(1)}, u32[]{:S(2)}, u32[]{:S(2)}) async-start(bf16[16,144,256]{2,1,0:T(8,128)(2,1)} %bitcast.4), calls=%async_computation | async-start | bytes 2359296 | tf_op jit(solution)/shard_map/all_to_all | solution.py:484
  28.2 12.7 %copy-start.3 = (bf16[1,128,2048]{2,1,0:T(8,128)(2,1)S(1)}, bf16[1,128,2048]{2,1,0:T(8,128)(2,1)}, u32[]{:S(2)}) copy-start(bf16[1,128,2048]{2,1,0:T(8,128)(2,1)} %param.18) | copy-start | bytes 1572868
  28.2 12.7 %copy-start.4 = (f32[2048]{0:T(1024)S(1)}, f32[2048]{0:T(1024)}, u32[]{:S(2)}) copy-start(f32[2048]{0:T(1024)} %param.29) | copy-start | bytes 24580
  28.2 12.8 %copy-start.5 = (f32[1024]{0:T(1024)S(1)}, f32[1024]{0:T(1024)}, u32[]{:S(2)}) copy-start(f32[1024]{0:T(1024)} %param.27) | copy-start | bytes 12292
  41.0 39.7 %copy-start.2 = (bf16[1,512,2048]{2,1,0:T(8,128)(2,1)S(1)}, bf16[1,512,2048]{2,1,0:T(8,128)(2,1)}, u32[]{:S(2)}) copy-start(bf16[1,512,2048]{2,1,0:T(8,128)(2,1)} %down_weight.1) | copy-start | bytes 6291460
  42.6 38.0 %copy-start = (bf16[1,2048,512]{2,1,0:T(8,128)(2,1)S(1)}, bf16[1,2048,512]{2,1,0:T(8,128)(2,1)}, u32[]{:S(2)}) copy-start(bf16[1,2048,512]{2,1,0:T(8,128)(2,1)} %gate_weight.1) | copy-start | bytes 6291460
  42.7 38.0 %copy-start.1 = (bf16[1,2048,512]{2,1,0:T(8,128)(2,1)S(1)}, bf16[1,2048,512]{2,1,0:T(8,128)(2,1)}, u32[]{:S(2)}) copy-start(bf16[1,2048,512]{2,1,0:T(8,128)(2,1)} %up_weight.1) | copy-start | bytes 6291460

commit v7 on v6

--- a/solution.py
+++ b/solution.py
@@ -378,19 +378,21 @@
     ).astype(jnp.bfloat16)
 
 
-def unstack(blocks, rows_out):
-    pairs, width = blocks.shape[0] // 16, blocks.shape[1]
-    view = blocks[...].astype(jnp.float32).reshape(pairs, 2, 8, width)
+def unstack(blocks, rows_out, lanes):
+    pairs, width = blocks.shape[0] // 16, lanes.stop - lanes.start
+    view = blocks[:, lanes].astype(jnp.float32).reshape(pairs, 2, 8, width)
     one, two = view[:, 0], view[:, 1]
     upper = lax.broadcasted_iota(jnp.int32, (pairs, 8, width), 1) < 4
     low = jnp.where(upper, one, pltpu.roll(two, 4, 1))
     high = jnp.where(upper, pltpu.roll(one, 4, 1), two)
-    rows_out[:, 0:width] = low.reshape(pairs * 8, width).astype(jnp.bfloat16)
-    rows_out[:, width : 2 * width] = high.reshape(pairs * 8, width).astype(jnp.bfloat16)
+    spans = [slice(lanes.start + at, lanes.stop + at) for at in (0, blocks.shape[1])]
+    rows_out[:, spans[0]] = low.reshape(pairs * 8, width).astype(jnp.bfloat16)
+    rows_out[:, spans[1]] = high.reshape(pairs * 8, width).astype(jnp.bfloat16)
+    return spans
 
 
 def expert_kernel(arrived, gate_weight, up_weight, down_weight, out, rows_in):
-    unstack(arrived, rows_in)
+    unstack(arrived, rows_in, slice(0, arrived.shape[1]))
     gate_act = jnp.dot(rows_in[...], gate_weight[0], preferred_element_type=jnp.float32)
     upward = jnp.dot(rows_in[...], up_weight[0], preferred_element_type=jnp.float32)
     hidden = (jax.nn.silu(gate_act) * upward).astype(jnp.bfloat16)
@@ -406,25 +408,37 @@
     out[...] = both.reshape(rows * 2, width).astype(jnp.bfloat16)
 
 
-def combine_kernel(returned, gather, stream, route_weight, out, rows_back):
-    unstack(returned, rows_back)
+def combine_kernel(
+    returned, gather, stream, route_weight, out, rows_back, result, departures
+):
     tokens = stream.shape[0]
-    picked = jnp.dot(gather[...], rows_back[...], preferred_element_type=jnp.float32)
-    routed = route_weight[:, 0:1] * picked[:tokens] + route_weight[:, 1:2] * picked[tokens:]
-    out[...] = (stream[...] + routed).astype(jnp.bfloat16)
+    moves = []
+    for at in range(0, returned.shape[1], 512):
+        for span in unstack(returned, rows_back, slice(at, at + 512)):
+            picked = jnp.dot(gather[...], rows_back[:, span], preferred_element_type=jnp.float32)
+            routed = route_weight[:, 0:1] * picked[:tokens] + route_weight[:, 1:2] * picked[tokens:]
+            result[:, span] = (stream[:, span] + routed).astype(jnp.bfloat16)
+            moves.append(
+                pltpu.make_async_copy(
+                    result.at[:, span], out.at[:, span], departures.at[len(moves)]
+                )
+            )
+            moves[-1].start()
+    for move in moves:
+        move.wait()
 
 
 VMEM = pl.BlockSpec(memory_space=pltpu.VMEM)
 HBM = pl.BlockSpec(memory_space=pltpu.HBM)
 
 
-def call(body, in_specs, out_shapes, mib, scratch=(), name=None):
+def call(body, in_specs, out_shapes, mib, scratch=(), name=None, out_spec=VMEM):
     many = isinstance(out_shapes, tuple)
     run = pl.pallas_call(
         body,
         in_specs=in_specs,
         out_shape=out_shapes,
-        out_specs=tuple(VMEM for _ in out_shapes) if many else VMEM,
+        out_specs=tuple(out_spec for _ in out_shapes) if many else out_spec,
         scratch_shapes=list(scratch),
         compiler_params=pltpu.CompilerParams(vmem_limit_bytes=mib * 2**20),
         name=name,
@@ -569,8 +583,13 @@
         [VMEM] * 4,
         shape((tokens, width), half),
         14,
-        scratch=(pltpu.VMEM((512, width), half),),
+        scratch=(
+            pltpu.VMEM((512, width), half),
+            pltpu.VMEM((tokens, width), half),
+            pltpu.SemaphoreType.DMA((4,)),
+        ),
         name="combine",
+        out_spec=HBM,
     )(returned, gather, stream, route_weight)[None]
 
 

time: 121 us -> 121 us (level)
  no operation moved by 1% of the time
where the time goes in v7:
time: 121 us; the launch traced here: 120 us
  blocking collectives  72.4 us (60%)
  Pallas kernels  24.4 us (20%)
  waiting for transfers between devices  13.7 us (11%)
  starting transfers between devices  8.6 us (7%)
    all_to_all x1, blocking collectives, per_device(): lax.all_to_all(outgoing, ('sp', 'dp'), split_axis=0, concat_axis=0, tiled...  38 us
    all_to_all x1, blocking collectives, per_device(): lax.all_to_all(answers, ('sp', 'dp'), split_axis=0, concat_axis=0, tiled=...  34.4 us
    pallas_call x6, Pallas kernels, placed(): run(*(pltpu.with_memory_space_constraint(x, pltpu.HBM) if spec is HBM els...  24.4 us
    all_to_all x1, waiting for transfers between devices, per_device(): lax.all_to_all(packed, 'sp', split_axis=0, concat_axis=0, tiled=True)  13.7 us
    all_to_all x1, starting transfers between devices, per_device(): lax.all_to_all(packed, 'sp', split_axis=0, concat_axis=0, tiled=True)  8.6 us
  transfers between devices with their start and end apart: 1, of which 1 were waited for; matrix products, arithmetic and copies ran while one was open for 1% of the time, Pallas kernels for 2%

profile of v7, /device:TPU:1, one launch (start us, length us, event | category | flops | bytes accessed | tf_op | source)
XLA Modules:
  0.0 120.4 jit_solution(12562425758213747424)
XLA Ops:
  0.0 0.0 copy-start.7
  0.0 2.1 %pack.1 = bf16[2304,256]{1,0:T(8,128)(2,1)} custom-call(bf16[128,256]{1,0:T(8,128)(2,1)} %bitcast.37, bf16[32,128]{1,0:T(8,128)(2,1)} %bitcast.38, f32[1,256]{1,0:T(1,128)} %bitcast.39), custom_call_target="tpu_custom_call" | custom-call | tf_op jit(solution)/shard_map/pack/pallas_call | solution.py:448
  2.2 0.0 copy-start.6
  2.2 8.6 %all-to-all-start = ((bf16[16,144,256]{2,1,0:T(8,128)(2,1)}), bf16[16,144,256]{2,1,0:T(8,128)(2,1)S(1)}, u32[]{:S(2)}, u32[]{:S(2)}) async-start(bf16[16,144,256]{2,1,0:T(8,128)(2,1)} %bitcast.4), calls=%async_computation | async-start | bytes 2359296 | tf_op jit(solution)/shard_map/all_to_all | solution.py:498
  10.8 0.0 copy-done.10
  10.8 0.1 copy.21.key_gain
  10.9 0.3 multiply_sine_fusion.1
  11.2 0.0 copy-done.8
  11.3 0.0 copy-done.9
  11.3 0.0 copy-done.7
  11.3 2.7 %query.1 = (bf16[2048,128]{1,0:T(8,128)(2,1)S(1)}, bf16[1024,256]{1,0:T(8,128)(2,1)S(1)}, bf16[1024,256]{1,0:T(8,128)(2,1)S(1)}, bf16[256,512]{1,0:T(8,128)(2,1)S(1)}, f32[128,2]{1,0:T(8,128)S(1)}) custom-call(bf16[128,1536]{1,0:T(8,128)(2,1)} %bitcast.36, f32[1,96]{1,0:T(1,128)} %bitcast.32, bf16[256,1024]{1,0:T(8,128)(2,1)} %key_weight.1, ...), custom_call_target="tpu_custom_call" | custom-call | tf_op jit(solution)/shard_map/query/pallas_call | solution.py:448
  14.0 0.5 multiply_sine_fusion
  14.5 13.7 %all-to-all-done = bf16[16,144,256]{2,1,0:T(8,128)(2,1)S(1)} async-done(((bf16[16,144,256]{2,1,0:T(8,128)(2,1)}), bf16[16,144,256]{2,1,0:T(8,128)(2,1)S(1)}, u32[]{:S(2)}, u32[]{:S(2)}) %all-to-all-start) | async-done | bytes 1179680 | tf_op jit(solution)/shard_map/all_to_all | solution.py:498
  28.2 0.0 copy-done.6
  28.2 12.7 %attend.1 = (bf16[128,1024]{1,0:T(8,128)(2,1)S(1)}, bf16[1024,2048]{1,0:T(8,128)(2,1)S(1)}) custom-call(bf16[2304,256]{1,0:T(8,128)(2,1)S(1)} %bitcast.27, bf16[2048,128]{1,0:T(8,128)(2,1)S(1)} %get-tuple-element.14.query, bf16[1024,256]{1,0:T(8,128)(2,1)S(1)} %get-tuple-element.15.key_weight_turned, f32[1,96]{1,0:T(1,128)S(1)} %bitcast.33, ...), custom_call_target="tpu_custom_call" | custom-call | tf_op jit(solution)/shard_map/attend/pallas_call | solution.py:448
  41.0 0.0 copy-start.2
  41.0 1.6 %mix.1 = (f32[128,2048]{1,0:T(8,128)S(1)}, bf16[1024,1024]{1,0:T(8,128)(2,1)S(1)}) custom-call(bf16[128,1024]{1,0:T(8,128)(2,1)S(1)} %get-tuple-element.16.heads_out, bf16[128,2048]{1,0:T(8,128)(2,1)S(1)} %bitcast.29, f32[1,1024]{1,0:T(1,128)S(1)} %bitcast.31, bf16[1024,2048]{1,0:T(8,128)(2,1)S(1)} %get-tuple-element.17.out_weight, f32[1,2048]{1,0:T(1,128)S(1)} %bitcast.30, ...), custom_call_target="tpu_custom_call" | custom-call | tf_op jit(solution)/shard_map/mix/pallas_call | solution.py:448
  42.6 0.0 copy-start
  42.7 0.0 copy-start.1
  42.7 38.0 %all_to_all.33 = bf16[128,8,1024]{2,1,0:T(8,128)(2,1)S(1)} all-to-all(bf16[128,8,1024]{2,1,0:T(8,128)(2,1)S(1)} %bitcast.28), channel_id=1, replica_groups=mesh['sp'=16,'dp'=8] {'sp','dp'}, dimensions={0} | all-to-all | bytes 4194304 | tf_op jit(solution)/shard_map/all_to_all | solution.py:571
  80.7 0.0 copy-done.1
  80.7 3.5 %expert.1 = bf16[1024,1024]{1,0:T(8,128)(2,1)S(1)} custom-call(bf16[1024,1024]{1,0:T(8,128)(2,1)S(1)} %bitcast.24, bf16[1,2048,512]{2,1,0:T(8,128)(2,1)S(1)} %copy-done, bf16[1,2048,512]{2,1,0:T(8,128)(2,1)S(1)} %copy-done.1, bf16[1,512,2048]{2,1,0:T(8,128)(2,1)S(1)} %copy-done.2), custom_call_target="tpu_custom_call" | custom-call | tf_op jit(solution)/shard_map/expert/pallas_call | solution.py:448
  84.2 34.4 %all_to_all.34 = bf16[128,8,1024]{2,1,0:T(8,128)(2,1)S(1)} all-to-all(bf16[128,8,1024]{2,1,0:T(8,128)(2,1)S(1)} %bitcast.25), channel_id=1, replica_groups=mesh['sp'=16,'dp'=8] {'sp','dp'}, dimensions={0} | all-to-all | bytes 4194304 | tf_op jit(solution)/shard_map/all_to_all | solution.py:580
  118.6 1.7 %combine.1 = bf16[128,2048]{1,0:T(8,128)(2,1)} custom-call(bf16[1024,1024]{1,0:T(8,128)(2,1)S(1)} %bitcast.26, bf16[256,512]{1,0:T(8,128)(2,1)S(1)} %get-tuple-element.20.gather, f32[128,2048]{1,0:T(8,128)S(1)} %get-tuple-element.21.stream, f32[128,2]{1,0:T(8,128)S(1)} %get-tuple-element.22.route_weight), custom_call_target="tpu_custom_call" | custom-call | tf_op jit(solution)/shard_map/combine/pallas_call | solution.py:448
  (14 shorter events, 0.0 us)
Async XLA Ops:
  0.0 10.8 %copy-start.10 = (f32[96]{0:T(128)S(1)}, f32[96]{0:T(128)}, u32[]{:S(2)}) copy-start(f32[96]{0:T(128)} %param.24) | copy-start | bytes 1156
  0.0 11.2 %copy-start.8 = (f32[1,128,2]{1,2,0:T(2,128)S(1)}, f32[1,128,2]{1,2,0:T(2,128)}, u32[]{:S(2)}) copy-start(f32[1,128,2]{1,2,0:T(2,128)} %param.32) | copy-start | bytes 3076
  0.0 11.2 %copy-start.9 = (f32[1,128]{1,0:T(1,128)S(1)}, f32[1,128]{1,0:T(1,128)}, u32[]{:S(2)}) copy-start(f32[1,128]{1,0:T(1,128)} %group_prob.1) | copy-start | bytes 1540
  0.0 11.3 %copy-start.7 = (s32[1,128,2]{1,2,0:T(2,128)S(1)}, s32[1,128,2]{1,2,0:T(2,128)}, u32[]{:S(2)}) copy-start(s32[1,128,2]{1,2,0:T(2,128)} %param.30) | copy-start | bytes 3076
  2.2 26.1 %copy-start.6 = (f32[96]{0:T(128)S(1)}, f32[96]{0:T(128)}, u32[]{:S(2)}) copy-start(f32[96]{0:T(128)} %param.23) | copy-start | bytes 1156
  2.2 26.1 %all-to-all-start = ((bf16[16,144,256]{2,1,0:T(8,128)(2,1)}), bf16[16,144,256]{2,1,0:T(8,128)(2,1)S(1)}, u32[]{:S(2)}, u32[]{:S(2)}) async-start(bf16[16,144,256]{2,1,0:T(8,128)(2,1)} %bitcast.4), calls=%async_computation | async-start | bytes 2359296 | tf_op jit(solution)/shard_map/all_to_all | solution.py:498
  28.2 12.7 %copy-start.3 = (bf16[1,128,2048]{2,1,0:T(8,128)(2,1)S(1)}, bf16[1,128,2048]{2,1,0:T(8,128)(2,1)}, u32[]{:S(2)}) copy-start(bf16[1,128,2048]{2,1,0:T(8,128)(2,1)} %param.18) | copy-start | bytes 1572868
  28.2 12.7 %copy-start.4 = (f32[2048]{0:T(1024)S(1)}, f32[2048]{0:T(1024)}, u32[]{:S(2)}) copy-start(f32[2048]{0:T(1024)} %param.29) | copy-start | bytes 24580
  28.2 12.8 %copy-start.5 = (f32[1024]{0:T(1024)S(1)}, f32[1024]{0:T(1024)}, u32[]{:S(2)}) copy-start(f32[1024]{0:T(1024)} %param.27) | copy-start | bytes 12292
  41.0 39.7 %copy-start.2 = (bf16[1,512,2048]{2,1,0:T(8,128)(2,1)S(1)}, bf16[1,512,2048]{2,1,0:T(8,128)(2,1)}, u32[]{:S(2)}) copy-start(bf16[1,512,2048]{2,1,0:T(8,128)(2,1)} %down_weight.1) | copy-start | bytes 6291460
  42.6 38.0 %copy-start = (bf16[1,2048,512]{2,1,0:T(8,128)(2,1)S(1)}, bf16[1,2048,512]{2,1,0:T(8,128)(2,1)}, u32[]{:S(2)}) copy-start(bf16[1,2048,512]{2,1,0:T(8,128)(2,1)} %gate_weight.1) | copy-start | bytes 6291460
  42.7 38.0 %copy-start.1 = (bf16[1,2048,512]{2,1,0:T(8,128)(2,1)S(1)}, bf16[1,2048,512]{2,1,0:T(8,128)(2,1)}, u32[]{:S(2)}) copy-start(bf16[1,2048,512]{2,1,0:T(8,128)(2,1)} %up_weight.1) | copy-start | bytes 6291460
